TPU v7x, 128 devices: a whole 4x4x4 slice. The times are simulated.
128 devices in a mesh: rep: 2 (over z_hi), fs: 32 (over z_lo, y, x), tp: 2 (over core).
Axes of the slice: x: 4, y: 4, z: 4 (z_hi: 2, z_lo: 2; z = z_hi * 2 + z_lo), core: 2. Of those that a mesh axis runs over, the one named last changes fastest.
Arguments:
- stream_in: bfloat16 [64, 1024, 2048], P(('rep', 'fs'), None, 'tp'), may hold values from -48 to 48
- decay_shift: float32 [64, 1024], P(('rep', 'fs')), may hold values from -1.5 to 0, as said below
- mixer_gain: float32 [2048], replicated, may hold values from 0.1 to 1.9
- gate_weight: bfloat16 [2048, 1024], P('fs', 'tp'), may hold values from -0.125 to 0.125
- input_weight: bfloat16 [2048, 1024], P('fs', 'tp'), may hold values from -0.125 to 0.125
- filter_taps: float32 [4, 1024], P(None, 'tp'), may hold values from -3 to 3
- recur_gate: bfloat16 [4, 256, 256], P('tp'), may hold values from -0.375 to 0.375
- inlet_gate: bfloat16 [4, 256, 256], P('tp'), may hold values from -0.375 to 0.375
- decay_param: float32 [1024], P('tp'), may hold values from 1.5 to 12
- mixer_out: bfloat16 [1024, 2048], P('tp', 'fs'), may hold values from -0.1875 to 0.1875
- feedforward_gain: float32 [2048], replicated, may hold values from 0.1 to 1.9
- up_weight: bfloat16 [2048, 4096], P('fs', 'tp'), may hold values from -0.125 to 0.125
- down_weight: bfloat16 [4096, 2048], P('tp', 'fs'), may hold values from -0.09375 to 0.09375
- final_gain: float32 [2048], P('tp'), may hold values from 0.1 to 1.9
Outputs:
- layer_out: bfloat16 [64, 1024, 2048], P(('rep', 'fs'), None, 'tp')
Inputs may be any that keep to these rules, and one draw needn't show every extreme that they name: `decay_shift`: every entry is negative.
All inputs are finite; a program needn't handle non-finite values.
Results may differ from a plain program's by a relative error of at most 0.015.
Values may be sent and summed in bfloat16 or wider, within the bound.
No kernel may reach another device: no remote copies, remote signals or barrier semaphores. Data moves between devices by JAX's collectives and lax.ppermute only.
A program may use at most 128 MiB of HBM per device.

v0:
```python
import functools

import jax
import jax.numpy as jnp
from jax import lax
from jax.experimental import pallas as pl
from jax.experimental.pallas import tpu as pltpu
from jax.sharding import Mesh, PartitionSpec as P

D = 2048
HALF = 1024
ROWS = 64
TILE = 256
SEGS = 8

epsilon = 1e-06
rate_scale = 8.0


f32, bf16 = jnp.float32, jnp.bfloat16
VMEM = pl.BlockSpec(memory_space=pltpu.VMEM)
HBM = pl.BlockSpec(memory_space=pltpu.HBM)
SMEM = pl.BlockSpec(memory_space=pltpu.SMEM)


def step(v, axis, shift):
    size = 2 if axis == "tp" else 4
    over = ("rep", "z") if axis == "z" else axis
    return lax.ppermute(v, over, [(i, (i + shift) % size) for i in range(size)])


def moved(places, axis, by):
    at = "xyz".index(axis)
    return [p[:at] + (p[at] + by,) + p[at + 1 :] for p in places]


def both_planes(shard):
    half = shard.shape[0] // 2
    lower = step(shard[:half], "z", 1)
    upper = step(shard[half:], "z", 3)
    pair = jnp.stack([shard, jnp.concatenate([lower, upper], axis=0)])
    return pair, [(0, 0, 0, 0, 0), (0, 0, 1, 0, 0)]


def ring_pieces(v, places, axis):
    far = step(v, axis, 2)
    left = step(v, axis, 1)
    right = step(v, axis, 3)
    return [
        (v, places),
        (left, moved(places, axis, -1)),
        (right, moved(places, axis, 1)),
        (far, moved(places, axis, 2)),
    ]


def whole_ring(v, places, axis):
    pieces = ring_pieces(v, places, axis)
    return jnp.concatenate([p for p, _ in pieces], axis=0), sum((q for _, q in pieces), [])


def plane_pieces(own, first, width):
    half = own.shape[0] // 2
    places = [(i % 4, i // 4, 0, 1, 0) for i in range(2 * half)]
    lower = step(own[:half, :, first : first + width], "z", 1)
    upper = step(own[half:, :, first : first + width], "z", 3)
    far = moved(places, "z", 1)
    return [(own, places, first), (lower, far[:half]), (upper, far[half:])]


def start_weights(refs, layout, pos, target, sem, plane=None):
    x, y, z, tp = pos[0], pos[1], pos[2], pos[3]
    for ref, (places, first_col, width, source_col) in zip(refs, layout):
        cols, source = pl.ds(first_col, width), pl.ds(source_col, width)
        for b, (px, py, pz, absolute, first_row) in enumerate(places):
            line = (py * 4 + px) if absolute else ((y + py) & 3) * 4 + ((x + px) & 3)
            at = line * ROWS + first_row
            if plane is None:
                at = ((z + pz + tp) & 1) * HALF + at
            elif pz != plane:
                continue
            at = at if isinstance(at, int) else pl.multiple_of(at, 16)
            pltpu.make_async_copy(
                ref.at[b, :, source], target.at[pl.ds(at, ref.shape[1]), cols], sem
            ).start()


def norm_kernel(own, other, gain, normed):
    def rows(i, _):
        s = pl.ds(pl.multiple_of(i * TILE, TILE), TILE)
        a, b = own[s, :].astype(f32), other[s, :].astype(f32)
        ms = (jnp.sum(a * a, -1, keepdims=True) + jnp.sum(b * b, -1, keepdims=True)) / D
        r = lax.rsqrt(ms + epsilon)
        normed[s, :HALF] = (a * r * gain[:, :HALF]).astype(bf16)
        normed[s, HALF:] = (b * r * gain[:, HALF:]).astype(bf16)
        return 0

    lax.fori_loop(0, own.shape[0] // TILE, rows, 0)


def project_kernel(layout, *refs):
    n = len(layout)
    pos, normed = refs[:2]
    pieces, (gate, inner) = refs[2 : 2 + n], refs[2 + n : 4 + n]
    weights, sem = refs[4 + n :]
    length, channels = gate.shape
    start_weights(pieces, layout, pos, weights, sem)
    pltpu.make_async_copy(weights, weights, sem).wait()
    for r in range(0, length, TILE):
        x = normed[r : r + TILE, :]
        both = jnp.dot(x, weights[...], preferred_element_type=f32).astype(bf16)
        gate[r : r + TILE, :] = both[:, :channels]
        inner[r : r + TILE, :] = both[:, channels:]


def mixer_kernel(layout, *refs):
    n = len(layout)
    pos, gate, inner, taps, recur_gate, inlet_gate, rate, shift = refs[:8]
    pieces, part_out = refs[8 : 8 + n], refs[8 + n]
    padded, decay, drive, prod, weights, part, weight_sem, out_sem = refs[9 + n :]
    length, channels = gate.shape
    start_weights(pieces, layout, pos, weights, weight_sem)
    padded[:8, :] = jnp.zeros((8, channels), f32)
    blocks, block = recur_gate.shape[0], recur_gate.shape[1]
    for r in range(0, length, TILE):
        padded[8 + r : 8 + r + TILE, :] = inner[r : r + TILE, :].astype(f32)
        acc = padded[r + 5 : r + 5 + TILE, :] * taps[0:1, :]
        for k in range(1, 4):
            acc = acc + padded[r + 5 + k : r + 5 + k + TILE, :] * taps[k : k + 1, :]
        filt = acc.astype(bf16)
        for n_b in range(blocks):
            cols = slice(n_b * block, (n_b + 1) * block)
            fb = filt[:, cols]
            recur = jax.nn.sigmoid(jnp.dot(fb, recur_gate[n_b], preferred_element_type=f32))
            inlet = jax.nn.sigmoid(jnp.dot(fb, inlet_gate[n_b], preferred_element_type=f32))
            log_decay = shift[r : r + TILE, :] - recur * rate[:, cols]
            a = jnp.exp(log_decay)
            t = 2.0 * log_decay
            series = -t * (
                1.0
                + t
                * (
                    1.0 / 2
                    + t
                    * (1.0 / 6 + t * (1.0 / 24 + t * (1.0 / 120 + t * (1.0 / 720 + t / 5040))))
                )
            )
            gone = jnp.where(t > -0.4, series, 1.0 - a * a)
            into = jnp.sqrt(gone) * inlet * fb.astype(f32)
            for q in range(block // 128):
                at = n_b * (block // 128) + q
                decay[at, r : r + TILE, :] = a[:, q * 128 : q * 128 + 128]
                drive[at, r : r + TILE, :] = into[:, q * 128 : q * 128 + 128]
    seg = length // SEGS

    def scan(j, carry):
        h, p = carry
        s = pl.ds(j, SEGS, stride=seg)
        hs, ps = [], []
        for q in range(channels // 128):
            a = decay[q, s, :]
            hq = a * h[q] + drive[q, s, :]
            pq = a * p[q]
            drive[q, s, :] = hq
            prod[q, s, :] = pq
            hs.append(hq)
            ps.append(pq)
        return tuple(hs), tuple(ps)

    lanes = channels // 128
    zero, one = jnp.zeros((SEGS, 128), f32), jnp.ones((SEGS, 128), f32)
    lax.fori_loop(0, seg, scan, ((zero,) * lanes, (one,) * lanes), unroll=8)
    carry = [jnp.zeros((1, 128), f32)] * lanes
    pltpu.make_async_copy(weights, weights, weight_sem).wait()
    for r in range(0, length, TILE):
        rows = []
        for i in range(r, r + TILE, seg):
            s = slice(i, i + seg)
            row = []
            for q in range(lanes):
                states = drive[q, s, :] + prod[q, s, :] * carry[q]
                carry[q] = states[seg - 1 : seg, :]
                branch = jax.nn.gelu(
                    gate[s, q * 128 : q * 128 + 128].astype(f32), approximate=True
                )
                row.append((states * branch).astype(bf16))
            rows.append(jnp.concatenate(row, axis=1))
        left = jnp.concatenate(rows, axis=0)
        s = slice(r, r + TILE)
        for h in range(2):
            half = weights[h * HALF : h * HALF + HALF, :]
            part[h, s, :] = dot_turned(left, half).astype(bf16)
            pltpu.make_async_copy(part.at[h, s, :], part_out.at[h, s, :], out_sem).start()
    pltpu.make_async_copy(part, part_out, out_sem).wait()


def turned_kernel(layout, plane, *refs):
    n = len(layout)
    pos, left_in = refs[:2]
    pieces, out_ref = refs[2 : 2 + n], refs[2 + n]
    left, weights, out, sem, in_sem, out_sem = refs[3 + n :]
    tiles = out.shape[0] // TILE

    def arriving(t):
        s = pl.ds(pl.multiple_of(t * TILE, TILE), TILE)
        return pltpu.make_async_copy(left_in.at[s, :], left.at[s, :], in_sem.at[t])

    arriving(0).start()
    start_weights(pieces, layout, pos, weights, sem, plane)
    for t in range(1, tiles):
        arriving(t).start()
    pltpu.make_async_copy(weights, weights, sem).wait()

    def rows(t, _):
        arriving(t).wait()
        s = pl.ds(pl.multiple_of(t * TILE, TILE), TILE)
        out[s, :] = dot_turned(left[s, :], weights[...]).astype(bf16)
        pltpu.make_async_copy(out.at[s, :], out_ref.at[s, :], out_sem).start()
        return 0

    lax.fori_loop(0, tiles, rows, 0)
    pltpu.make_async_copy(out, out_ref, out_sem).wait()


def dot_turned(left, right):
    return lax.dot_general(left, right, (((1,), (1,)), ((), ())), preferred_element_type=f32)


def ffn_kernel(layout, *refs):
    pos, own, other, mine, theirs, gain = refs[:6]
    n = len(layout)
    pieces, (mid_out, act_out) = refs[6 : 6 + n], refs[6 + n : 8 + n]
    stream, parts, up, normed, mid, act, up_sem, in_sem, out_sem, mid_sem = refs[8 + n :]
    tiles = own.shape[0] // TILE

    def arriving(t):
        s = pl.ds(pl.multiple_of(t * TILE, TILE), TILE)
        pairs = [
            (own, stream.at[0]),
            (other, stream.at[1]),
            (mine.at[0], parts.at[0, 0]),
            (theirs.at[1], parts.at[0, 1]),
            (mine.at[1], parts.at[1, 0]),
            (theirs.at[0], parts.at[1, 1]),
        ]
        return [
            pltpu.make_async_copy(src.at[s, :], dst.at[s, :], in_sem.at[t, k])
            for k, (src, dst) in enumerate(pairs)
        ]

    def norm(t):
        s = pl.ds(pl.multiple_of(t * TILE, TILE), TILE)
        halves = []
        for h in range(2):
            v = stream[h, s, :].astype(f32) + (
                parts[h, 0, s, :].astype(f32) + parts[h, 1, s, :].astype(f32)
            )
            v = v.astype(bf16)
            mid[s, h * HALF : h * HALF + HALF] = v
            halves.append(v.astype(f32))
        a, b = halves
        ms = (jnp.sum(a * a, -1, keepdims=True) + jnp.sum(b * b, -1, keepdims=True)) / D
        r = lax.rsqrt(ms + epsilon)
        normed[s, :HALF] = (a * r * gain[:, :HALF]).astype(bf16)
        normed[s, HALF:] = (b * r * gain[:, HALF:]).astype(bf16)

    for c in arriving(0):
        c.start()
    start_weights(pieces, layout, pos, up, up_sem)
    for t in range(1, tiles):
        for c in arriving(t):
            c.start()
    for c in arriving(0):
        c.wait()
    norm(0)
    pltpu.make_async_copy(up, up, up_sem).wait()

    def product(t):
        s = pl.ds(pl.multiple_of(t * TILE, TILE), TILE)
        prod = jnp.dot(normed[s, :], up[...], preferred_element_type=f32)
        act[s, :] = jnp.square(jnp.maximum(prod, 0.0)).astype(bf16)

    def leave(t):
        s = pl.ds(pl.multiple_of(t * TILE, TILE), TILE)
        pltpu.make_async_copy(mid.at[s, :], mid_out.at[s, :], mid_sem).start()
        pltpu.make_async_copy(act.at[s, :], act_out.at[s, :], out_sem).start()

    def rows(t, _):
        for c in arriving(t + 1):
            c.wait()
        norm(t + 1)
        product(t)
        leave(t)
        return 0

    lax.fori_loop(0, tiles - 1, rows, 0)
    product(tiles - 1)
    leave(tiles - 1)
    pltpu.make_async_copy(mid, mid_out, mid_sem).wait()
    pltpu.make_async_copy(act, act_out, out_sem).wait()


def closing_kernel(pos, mid, mine_a, theirs_a, mine_b, theirs_b, gain, out_ref, *scratch):
    stream, parts, out, in_sem, out_sem = scratch
    tiles = mid.shape[0] // TILE
    near = (pos[2] + pos[3]) & 1

    def arriving(t):
        s = slice(t * TILE, (t + 1) * TILE)
        pairs = [
            (mid, stream),
            (mine_a, parts.at[near, 0]),
            (theirs_a, parts.at[near, 1]),
            (mine_b, parts.at[1 - near, 0]),
            (theirs_b, parts.at[1 - near, 1]),
        ]
        return [
            pltpu.make_async_copy(src.at[s, :], dst.at[s, :], in_sem.at[t, k])
            for k, (src, dst) in enumerate(pairs)
        ]

    for t in range(tiles):
        for c in arriving(t):
            c.start()
    for t in range(tiles):
        for c in arriving(t):
            c.wait()
        for half in range(2):
            s = slice(t * TILE + half * 128, t * TILE + half * 128 + 128)
            a, b = [
                stream[s, h * HALF : h * HALF + HALF].astype(f32)
                + (parts[h, 0, s, :].astype(f32) + parts[h, 1, s, :].astype(f32))
                for h in range(2)
            ]
            ms = (jnp.sum(a * a, -1, keepdims=True) + jnp.sum(b * b, -1, keepdims=True)) / D
            out[s, :] = (a * lax.rsqrt(ms + epsilon) * gain[...]).astype(bf16)
        s = slice(t * TILE, (t + 1) * TILE)
        pltpu.make_async_copy(out.at[s, :], out_ref.at[s, :], out_sem).start()
    pltpu.make_async_copy(out, out_ref, out_sem).wait()


def cost(flops, moved_bytes):
    return pl.CostEstimate(flops=int(flops), bytes_accessed=int(moved_bytes), transcendentals=0)


def call(kernel, out_shapes, specs, flops, scratch=(), outs=VMEM):
    return pl.pallas_call(
        kernel,
        out_shape=out_shapes,
        in_specs=specs,
        out_specs=jax.tree.map(lambda _: outs, out_shapes),
        scratch_shapes=list(scratch),
        cost_estimate=cost(flops, 8e6),
        compiler_params=pltpu.CompilerParams(vmem_limit_bytes=56 * 2**20),
    )


def flat(pieces, first_col, width, source=0):
    layout = [
        (piece[1], first_col, width, piece[2] if len(piece) > 2 else source) for piece in pieces
    ]
    return [piece[0] for piece in pieces], layout


def local(
    stream_in,
    decay_shift,
    mixer_gain,
    gate_weight,
    input_weight,
    filter_taps,
    recur_gate,
    inlet_gate,
    decay_param,
    mixer_out,
    feedforward_gain,
    up_weight,
    down_weight,
    final_gain,
):
    num_seq, length, half = stream_in.shape
    channels = gate_weight.shape[1]
    hidden = up_weight.shape[1]
    assert num_seq == 1 and half == HALF
    tp = lax.axis_index("tp")
    pos = jnp.stack(
        [lax.axis_index("x"), lax.axis_index("y"), lax.axis_index("z"), tp]
    ).astype(jnp.int32)

    def own_first(gain):
        halves = gain.reshape(2, HALF)
        return jnp.where(tp == 0, halves, halves[::-1]).reshape(1, D)

    own = stream_in.reshape(length, half)
    other = step(own, "tp", 1)

    mid_col, part = hidden // 2, channels // 2
    mixer_t, down_t = mixer_out.T, down_weight.T
    here = [(0, 0, 0, 0, 0)]
    left = jnp.concatenate([gate_weight, mixer_t[:, :part]], axis=1)[None]
    right = jnp.concatenate([mixer_t[:, part:], input_weight], axis=1)[None]
    by_x = whole_ring(left, here, "x")
    by_y = whole_ring(right, here, "y")
    pair, places = both_planes(up_weight)
    by_xy = whole_ring(*by_x, "y")
    by_yx = whole_ring(*by_y, "x")
    x_pieces = [by_xy, (step(by_xy[0], "z", 1), moved(by_xy[1], "z", 1))]
    y_pieces = [by_yx, (step(by_yx[0], "z", 3), moved(by_yx[1], "z", 1))]
    later = whole_ring(pair[:, :, :mid_col], places, "y")
    up_x = ring_pieces(*later, "x")
    later = whole_ring(pair[:, :, mid_col:], places, "x")
    up_y = ring_pieces(*later, "y")
    down_t = lax.optimization_barrier((down_t, by_x[0], by_y[0]))[0]
    plane = lax.all_gather(down_t, ("y", "x"), axis=0, tiled=False)
    down_pieces = plane_pieces(plane, 0, hidden)

    shape = jax.ShapeDtypeStruct
    whole, one_half = shape((length, D), bf16), shape((length, HALF), bf16)
    normed = call(norm_kernel, whole, [VMEM] * 3, 2e9)(own, other, own_first(mixer_gain))

    a, la = flat(x_pieces, 0, channels)
    b, lb = flat(y_pieces, channels, channels, part)
    some = shape((length, channels), bf16)
    gate, inner = call(
        functools.partial(project_kernel, la + lb),
        (some, some),
        [SMEM, VMEM] + [HBM] * len(la + lb),
        4 * length * channels * D,
        [pltpu.VMEM((D, 2 * channels), bf16), pltpu.SemaphoreType.DMA],
    )(pos, normed, *a, *b)
    scan_buffer = pltpu.VMEM((channels // 128, length, 128), f32)
    a, la = flat(x_pieces, 0, part, channels)
    b, lb = flat(y_pieces, part, part)
    partial = shape((2, length, HALF), bf16)
    mine = call(
        functools.partial(mixer_kernel, la + lb),
        partial,
        [SMEM] + [VMEM] * 7 + [HBM] * len(la + lb),
        1.2e10,
        [
            pltpu.VMEM((length + 8, channels), f32),
            scan_buffer,
            scan_buffer,
            scan_buffer,
            pltpu.VMEM((D, channels), bf16),
            pltpu.VMEM((2, length, HALF), bf16),
            pltpu.SemaphoreType.DMA,
            pltpu.SemaphoreType.DMA,
        ],
        HBM,
    )(
        pos,
        gate,
        inner,
        filter_taps,
        recur_gate,
        inlet_gate,
        (rate_scale * jax.nn.softplus(-decay_param)).reshape(1, channels),
        decay_shift.reshape(length, 1),
        *a,
        *b,
    )
    theirs = step(mine, "tp", 1)
    tiles = length // TILE

    def turned(left, pieces, plane):
        arrays, layout = flat(pieces, 0, left.shape[1])
        return call(
            functools.partial(turned_kernel, layout, plane),
            one_half,
            [SMEM, HBM] + [HBM] * len(layout),
            2 * length * left.shape[1] * HALF,
            [
                pltpu.VMEM(left.shape, bf16),
                pltpu.VMEM((HALF, left.shape[1]), bf16),
                pltpu.VMEM((length, HALF), bf16),
                pltpu.SemaphoreType.DMA,
                pltpu.SemaphoreType.DMA((tiles,)),
                pltpu.SemaphoreType.DMA,
            ],
            HBM,
        )(pos, left, *arrays)

    a, la = flat(up_x, 0, mid_col)
    b, lb = flat(up_y, mid_col, mid_col)
    mid, activated = call(
        functools.partial(ffn_kernel, la + lb),
        (whole, shape((length, hidden), bf16)),
        [SMEM] + [HBM] * 4 + [VMEM] + [HBM] * len(la + lb),
        2 * length * hidden * D,
        [
            pltpu.VMEM((2, length, HALF), bf16),
            pltpu.VMEM((2, 2, length, HALF), bf16),
            pltpu.VMEM((D, hidden), bf16),
            pltpu.VMEM((length, D), bf16),
            pltpu.VMEM((length, D), bf16),
            pltpu.VMEM((length, hidden), bf16),
            pltpu.SemaphoreType.DMA,
            pltpu.SemaphoreType.DMA((tiles, 6)),
            pltpu.SemaphoreType.DMA,
            pltpu.SemaphoreType.DMA,
        ],
        HBM,
    )(pos, own, other, mine, theirs, own_first(feedforward_gain), *a, *b)
    mine_c = turned(activated, down_pieces[:1], 0)
    theirs_c = step(mine_c, "tp", 1)
    mine_d = turned(activated, down_pieces[1:], 1)
    theirs_d = step(mine_d, "tp", 1)
    out = call(
        closing_kernel,
        one_half,
        [SMEM] + [HBM] * 5 + [VMEM],
        2e9,
        [
            pltpu.VMEM((length, D), bf16),
            pltpu.VMEM((2, 2, length, HALF), bf16),
            pltpu.VMEM((length, HALF), bf16),
            pltpu.SemaphoreType.DMA((tiles, 5)),
            pltpu.SemaphoreType.DMA,
        ],
        HBM,
    )(pos, mid, mine_c, theirs_c, mine_d, theirs_d, final_gain.reshape(1, HALF))
    return out.reshape(num_seq, length, half)


def solution(mesh):
    grid = Mesh(mesh.devices.reshape(2, 2, 4, 4, 2), ("rep", "z", "y", "x", "tp"))
    fs = ("z", "y", "x")
    seqs = ("rep",) + fs
    return jax.shard_map(
        local,
        mesh=grid,
        in_specs=(
            P(seqs, None, "tp"),
            P(seqs, None),
            P(),
            P(fs, "tp"),
            P(fs, "tp"),
            P(None, "tp"),
            P("tp", None, None),
            P("tp", None, None),
            P("tp"),
            P("tp", fs),
            P(),
            P(fs, "tp"),
            P("tp", fs),
            P("tp"),
        ),
        out_specs=P(seqs, None, "tp"),
        check_vma=False,
    )
```

profile of v0, /device:TPU:1, one launch (start us, length us, event | category | flops | bytes accessed | tf_op | source)
XLA Modules:
  0.0 290.0 jit_solution(8875670278337924618)
XLA Ops:
  8.3 3.7 %collective-permute-start.10 = (bf16[1,64,768]{2,1,0:T(8,128)(2,1)S(1)}, bf16[1,64,768]{2,1,0:T(8,128)(2,1)S(1)}, u32[]{:S(2)}, u32[]{:S(2)}) collective-permute-start(bf16[1,64,768]{2,1,0:T(8,128)(2,1)S(1)} %maximum_bitcast_fusion.2), channel_id=1, source_target_pairs={{0,16},{8,24},{16,0},{24,8},{1,17},{9,25},{17,1},{25,9},{2,18},{10... | collective-permute-start | bytes 294920 | tf_op jit(solution)/shard_map/ppermute | solution.py:29
  20.3 4.0 %collective-permute-done.3 = bf16[1,64,768]{2,1,0:T(8,128)(2,1)S(1)} collective-permute-done((bf16[1,64,768]{2,1,0:T(8,128)(2,1)S(1)}, bf16[1,64,768]{2,1,0:T(8,128)(2,1)S(1)}, u32[]{:S(2)}, u32[]{:S(2)}) %collective-permute-start.3) | collective-permute-done | bytes 98336 | tf_op jit(solution)/shard_map/ppermute | solution.py:29
  35.0 6.3 %collective-permute-done.11 = bf16[4,64,768]{2,1,0:T(8,128)(2,1)S(1)} collective-permute-done((bf16[4,64,768]{2,1,0:T(8,128)(2,1)S(1)}, bf16[4,64,768]{2,1,0:T(8,128)(2,1)S(1)}, u32[]{:S(2)}, u32[]{:S(2)}) %collective-permute-start.11) | collective-permute-done | bytes 393248 | tf_op jit(solution)/shard_map/ppermute | solution.py:29
  43.6 8.6 %collective-permute-done.13 = bf16[4,64,768]{2,1,0:T(8,128)(2,1)S(1)} collective-permute-done((bf16[4,64,768]{2,1,0:T(8,128)(2,1)S(1)}, bf16[4,64,768]{2,1,0:T(8,128)(2,1)S(1)}, u32[]{:S(2)}, u32[]{:S(2)}) %collective-permute-start.13) | collective-permute-done | bytes 393248 | tf_op jit(solution)/shard_map/ppermute | solution.py:29
  53.0 4.0 %collective-permute-start.14 = (bf16[16,64,768]{2,1,0:T(8,128)(2,1)}, bf16[16,64,768]{2,1,0:T(8,128)(2,1)}, u32[]{:S(2)}, u32[]{:S(2)}) collective-permute-start(bf16[16,64,768]{2,1,0:T(8,128)(2,1)} %constant_dynamic-update-slice_fusion.7.refs_4_.refs_10_), channel_id=1, source_target_pairs={{0,96},{32,0},{64,32},{96,64},{1,97},{33,1},{65,33},{97,65},{2,98}... | collective-permute-start | bytes 4718600 | tf_op jit(solution)/shard_map/ppermute | solution.py:29
  62.5 6.0 %shard_map.136.refs_1_ = bf16[1024,2048]{1,0:T(8,128)(2,1)} custom-call(bf16[1024,1024]{1,0:T(8,128)(2,1)} %bitcast.34, bf16[1024,1024]{1,0:T(8,128)(2,1)} %collective-permute-done.other.refs_2_, f32[1,2048]{1,0:T(1,128)} %bitcast.40), custom_call_target="tpu_custom_call" | custom-call | flops 2000000000 | bytes 8000000 | tf_op jit(solution)/shard_map/pallas_call | solution.py:419
  68.5 21.7 %collective-permute-done.14.refs_5_.refs_11_ = bf16[16,64,768]{2,1,0:T(8,128)(2,1)} collective-permute-done((bf16[16,64,768]{2,1,0:T(8,128)(2,1)}, bf16[16,64,768]{2,1,0:T(8,128)(2,1)}, u32[]{:S(2)}, u32[]{:S(2)}) %collective-permute-start.14) | collective-permute-done | bytes 1572896 | tf_op jit(solution)/shard_map/ppermute | solution.py:29
  93.0 9.9 %shard_map.137 = (bf16[1024,512]{1,0:T(8,128)(2,1)}, bf16[1024,512]{1,0:T(8,128)(2,1)}) custom-call(s32[4]{0:T(128)} %pad_add_fusion.refs_0_.pos, bf16[1024,2048]{1,0:T(8,128)(2,1)} %shard_map.136.refs_1_, bf16[16,64,768]{2,1,0:T(8,128)(2,1)} %constant_dynamic-update-slice_fusion.refs_2_.refs_8_, ...), custom_call_target="tpu_custom_call" | custom-call | flops 4294967296 | bytes 8000000 | tf_op jit(solution)/shard_map/pallas_call | solution.py:424
  102.9 16.7 %shard_map.138.refs_3_ = bf16[2,1024,1024]{2,1,0:T(8,128)(2,1)} custom-call(s32[4]{0:T(128)} %pad_add_fusion.refs_0_.pos, bf16[1024,512]{1,0:T(8,128)(2,1)} %get-tuple-element.10.refs_1_, bf16[1024,512]{1,0:T(8,128)(2,1)} %get-tuple-element.11.refs_2_, f32[4,512]{1,0:T(4,128)} %refs_3_.1, bf16[2,256,256]{2,1,0:T(8,128)(2,1)} %refs_4_.1, ...), custom_call_target="tpu_custom_call" | custom-call | flops 12000000000 | bytes 8000000 | tf_op jit(solution)/shard_map/pallas_call | solution.py:435
  119.6 4.8 %collective-permute-start.15 = (bf16[2,1024,1024]{2,1,0:T(8,128)(2,1)}, bf16[2,1024,1024]{2,1,0:T(8,128)(2,1)}, u32[]{:S(2)}, u32[]{:S(2)}) collective-permute-start(bf16[2,1024,1024]{2,1,0:T(8,128)(2,1)} %shard_map.138.refs_3_), channel_id=1, source_target_pairs={{0,1},{1,0},{2,3},{3,2},{4,5},{5,4},{6,7},{7,6},{8,9},{9,8},{10,11... | collective-permute-start | bytes 12582920 | tf_op jit(solution)/shard_map/ppermute | solution.py:29
  127.1 3.6 %collective-permute-done.16 = bf16[32,2048]{1,0:T(8,128)(2,1)S(1)} collective-permute-done((bf16[32,2048]{1,0:T(8,128)(2,1)S(1)}, bf16[32,2048]{1,0:T(8,128)(2,1)S(1)}, u32[]{:S(2)}, u32[]{:S(2)}) %collective-permute-start.16) | collective-permute-done | bytes 131104 | tf_op jit(solution)/shard_map/ppermute | solution.py:29
  137.8 4.6 %collective-permute-done.18 = bf16[2,64,1024]{2,1,0:T(8,128)(2,1)S(1)} collective-permute-done((bf16[2,64,1024]{2,1,0:T(8,128)(2,1)S(1)}, bf16[2,64,1024]{2,1,0:T(8,128)(2,1)S(1)}, u32[]{:S(2)}, u32[]{:S(2)}) %collective-permute-start.18) | collective-permute-done | bytes 262176 | tf_op jit(solution)/shard_map/ppermute | solution.py:29
  142.4 4.5 %collective-permute-done.19 = bf16[2,64,1024]{2,1,0:T(8,128)(2,1)S(1)} collective-permute-done((bf16[2,64,1024]{2,1,0:T(8,128)(2,1)S(1)}, bf16[2,64,1024]{2,1,0:T(8,128)(2,1)S(1)}, u32[]{:S(2)}, u32[]{:S(2)}) %collective-permute-start.19) | collective-permute-done | bytes 262176 | tf_op jit(solution)/shard_map/ppermute | solution.py:29
  152.5 26.1 %collective-permute-done.25 = bf16[2,64,1024]{2,1,0:T(8,128)(2,1)S(1)} collective-permute-done((bf16[2,64,1024]{2,1,0:T(8,128)(2,1)S(1)}, bf16[2,64,1024]{2,1,0:T(8,128)(2,1)S(1)}, u32[]{:S(2)}, u32[]{:S(2)}) %collective-permute-start.25) | collective-permute-done | bytes 262176 | tf_op jit(solution)/shard_map/ppermute | solution.py:29
  185.1 4.9 %fusion.2 = (bf16[512,2048]{1,0:T(8,128)(2,1)}, bf16[512,2048]{1,0:T(8,128)(2,1)}) fusion(bf16[1024,2048]{1,0:T(8,128)(2,1)} %all-gather.3.cloned.1.call-done), kind=kLoop, calls=%fused_computation.30 | loop fusion | bytes 8388608 | tf_op jit(solution)/shard_map/slice | solution.py:66
  190.0 3.8 %collective-permute-done.23.refs_9_ = bf16[8,64,1024]{2,1,0:T(8,128)(2,1)} collective-permute-done((bf16[8,64,1024]{2,1,0:T(8,128)(2,1)S(1)}, bf16[8,64,1024]{2,1,0:T(8,128)(2,1)}, u32[]{:S(2)}, u32[]{:S(2)}) %collective-permute-start.23) | collective-permute-done | bytes 1048608 | tf_op jit(solution)/shard_map/ppermute | solution.py:29
  198.0 6.0 %collective-permute-done.28.refs_12_ = bf16[8,64,1024]{2,1,0:T(8,128)(2,1)} collective-permute-done((bf16[8,64,1024]{2,1,0:T(8,128)(2,1)S(1)}, bf16[8,64,1024]{2,1,0:T(8,128)(2,1)}, u32[]{:S(2)}, u32[]{:S(2)}) %collective-permute-start.28) | collective-permute-done | bytes 1048608 | tf_op jit(solution)/shard_map/ppermute | solution.py:29
  204.1 7.3 %collective-permute-done.29.refs_13_ = bf16[8,64,1024]{2,1,0:T(8,128)(2,1)} collective-permute-done((bf16[8,64,1024]{2,1,0:T(8,128)(2,1)S(1)}, bf16[8,64,1024]{2,1,0:T(8,128)(2,1)}, u32[]{:S(2)}, u32[]{:S(2)}) %collective-permute-start.29) | collective-permute-done | bytes 1048608 | tf_op jit(solution)/shard_map/ppermute | solution.py:29
  211.4 20.7 %shard_map.139 = (bf16[1024,2048]{1,0:T(8,128)(2,1)}, bf16[1024,2048]{1,0:T(8,128)(2,1)}) custom-call(s32[4]{0:T(128)} %pad_add_fusion.refs_0_.pos, bf16[1024,1024]{1,0:T(8,128)(2,1)} %bitcast.35, bf16[1024,1024]{1,0:T(8,128)(2,1)} %collective-permute-done.other.refs_2_, bf16[2,1024,1024]{2,1,0:T(8,128)(2,1)} %shard_map.138.refs_3_, ...), custom_call_target="tpu_custom_call" | custom-call | flops 8589934592 | bytes 8000000 | tf_op jit(solution)/shard_map/pallas_call | solution.py:486
  232.2 9.7 %shard_map.140.mine_a = bf16[1024,1024]{1,0:T(8,128)(2,1)} custom-call(s32[4]{0:T(128)} %pad_add_fusion.refs_0_.pos, bf16[1024,2048]{1,0:T(8,128)(2,1)} %get-tuple-element.13.refs_1_, bf16[16,64,2048]{2,1,0:T(8,128)(2,1)} %bitcast.33), custom_call_target="tpu_custom_call" | custom-call | flops 4294967296 | bytes 8000000 | tf_op jit(solution)/shard_map/pallas_call | solution.py:468
  241.9 18.5 %collective-permute-start.30 = (bf16[1024,1024]{1,0:T(8,128)(2,1)}, bf16[1024,1024]{1,0:T(8,128)(2,1)S(1)}, u32[]{:S(2)}, u32[]{:S(2)}) collective-permute-start(bf16[1024,1024]{1,0:T(8,128)(2,1)} %shard_map.140.mine_a), channel_id=1, source_target_pairs={{0,1},{1,0},{2,3},{3,2},{4,5},{5,4},{6,7},{7,6},{8,9},{9,8},{10,11... | collective-permute-start | bytes 6291464 | tf_op jit(solution)/shard_map/ppermute | solution.py:29
  260.3 9.7 %shard_map.141.mine_b = bf16[1024,1024]{1,0:T(8,128)(2,1)} custom-call(s32[4]{0:T(128)} %pad_add_fusion.refs_0_.pos, bf16[1024,2048]{1,0:T(8,128)(2,1)} %get-tuple-element.13.refs_1_, bf16[8,64,2048]{2,1,0:T(8,128)(2,1)} %collective-permute-done.31.refs_2_, bf16[8,64,2048]{2,1,0:T(8,128)(2,1)} %collective-permute-done.32.refs_3_), custom_call_target="tpu_custom_call" | custom-call | flops 4294967296 | bytes 8000000 | tf_op jit(solution)/shard_map/pallas_call | solution.py:468
  270.2 4.3 %collective-permute-done.33.theirs_b = bf16[1024,1024]{1,0:T(8,128)(2,1)S(1)} collective-permute-done((bf16[1024,1024]{1,0:T(8,128)(2,1)}, bf16[1024,1024]{1,0:T(8,128)(2,1)S(1)}, u32[]{:S(2)}, u32[]{:S(2)}) %collective-permute-start.33) | collective-permute-done | bytes 2097184 | tf_op jit(solution)/shard_map/ppermute | solution.py:29
  275.9 7.2 %shard_map.142 = bf16[1024,1024]{1,0:T(8,128)(2,1)} custom-call(s32[4]{0:T(128)} %pad_add_fusion.refs_0_.pos, bf16[1024,2048]{1,0:T(8,128)(2,1)} %get-tuple-element.12.mid, bf16[1024,1024]{1,0:T(8,128)(2,1)} %shard_map.140.mine_a, bf16[1024,1024]{1,0:T(8,128)(2,1)} %copy-done.1, bf16[1024,1024]{1,0:T(8,128)(2,1)} %shard_map.141.mine_b, ...), custom_call_target="tpu_custom_call" | custom-call | flops 2000000000 | bytes 8000000 | tf_op jit(solution)/shard_map/pallas_call | solution.py:509
  (113 shorter events, 59.6 us)
Async XLA Ops:
  6.5 178.5 %all-gather.3.cloned.1.call-start = ((), (), s32[]{:S(2)}) async-start(), calls=%async_computation | async-start | bytes 4456448 | tf_op jit(solution)/shard_map/all_gather | solution.py:414
  24.4 38.1 %collective-permute-start = (bf16[1024,1024]{1,0:T(8,128)(2,1)S(1)}, bf16[1024,1024]{1,0:T(8,128)(2,1)}, u32[]{:S(2)}, u32[]{:S(2)}) collective-permute-start(bf16[1024,1024]{1,0:T(8,128)(2,1)S(1)} %bitcast.36), channel_id=1, source_target_pairs={{0,1},{1,0},{2,3},{3,2},{4,5},{5,4},{6,7},{7,6},{8,9},{9,8},{10,11... | collective-permute-start | bytes 6291464 | tf_op jit(solution)/shard_map/ppermute | solution.py:29
  28.2 13.1 %collective-permute-start.11 = (bf16[4,64,768]{2,1,0:T(8,128)(2,1)S(1)}, bf16[4,64,768]{2,1,0:T(8,128)(2,1)S(1)}, u32[]{:S(2)}, u32[]{:S(2)}) collective-permute-start(bf16[4,64,768]{2,1,0:T(8,128)(2,1)S(1)} %pad_maximum_fusion.3), channel_id=1, source_target_pairs={{0,2},{2,4},{4,6},{6,0},{1,3},{3,5},{5,7},{7,1},{8,10},{10,12},{12... | collective-permute-start | bytes 1179656 | tf_op jit(solution)/shard_map/ppermute | solution.py:29
  28.2 14.6 %collective-permute-start.12 = (bf16[4,64,768]{2,1,0:T(8,128)(2,1)S(1)}, bf16[4,64,768]{2,1,0:T(8,128)(2,1)S(1)}, u32[]{:S(2)}, u32[]{:S(2)}) collective-permute-start(bf16[4,64,768]{2,1,0:T(8,128)(2,1)S(1)} %pad_maximum_fusion.3), channel_id=1, source_target_pairs={{0,6},{2,0},{4,2},{6,4},{1,7},{3,1},{5,3},{7,5},{8,14},{10,8},{12,... | collective-permute-start | bytes 1179656 | tf_op jit(solution)/shard_map/ppermute | solution.py:29
  30.9 21.4 %collective-permute-start.13 = (bf16[4,64,768]{2,1,0:T(8,128)(2,1)S(1)}, bf16[4,64,768]{2,1,0:T(8,128)(2,1)S(1)}, u32[]{:S(2)}, u32[]{:S(2)}) collective-permute-start(bf16[4,64,768]{2,1,0:T(8,128)(2,1)S(1)} %pad_maximum_fusion.3), channel_id=1, source_target_pairs={{0,4},{2,6},{4,0},{6,2},{1,5},{3,7},{5,1},{7,3},{8,12},{10,14},{12... | collective-permute-start | bytes 1179656 | tf_op jit(solution)/shard_map/ppermute | solution.py:29
  31.2 25.8 %collective-permute-start.4 = (bf16[4,64,768]{2,1,0:T(8,128)(2,1)S(1)}, bf16[4,64,768]{2,1,0:T(8,128)(2,1)S(1)}, u32[]{:S(2)}, u32[]{:S(2)}) collective-permute-start(bf16[4,64,768]{2,1,0:T(8,128)(2,1)S(1)} %pad_maximum_fusion.2), channel_id=1, source_target_pairs={{0,8},{8,16},{16,24},{24,0},{1,9},{9,17},{17,25},{25,1},{2,10},{10... | collective-permute-start | bytes 1179656 | tf_op jit(solution)/shard_map/ppermute | solution.py:29
  41.3 16.5 %collective-permute-start.5 = (bf16[4,64,768]{2,1,0:T(8,128)(2,1)S(1)}, bf16[4,64,768]{2,1,0:T(8,128)(2,1)S(1)}, u32[]{:S(2)}, u32[]{:S(2)}) collective-permute-start(bf16[4,64,768]{2,1,0:T(8,128)(2,1)S(1)} %pad_maximum_fusion.2), channel_id=1, source_target_pairs={{0,24},{8,0},{16,8},{24,16},{1,25},{9,1},{17,9},{25,17},{2,26},{10... | collective-permute-start | bytes 1179656 | tf_op jit(solution)/shard_map/ppermute | solution.py:29
  42.8 15.7 %collective-permute-start.6 = (bf16[4,64,768]{2,1,0:T(8,128)(2,1)S(1)}, bf16[4,64,768]{2,1,0:T(8,128)(2,1)S(1)}, u32[]{:S(2)}, u32[]{:S(2)}) collective-permute-start(bf16[4,64,768]{2,1,0:T(8,128)(2,1)S(1)} %pad_maximum_fusion.2), channel_id=1, source_target_pairs={{0,16},{8,24},{16,0},{24,8},{1,17},{9,25},{17,1},{25,9},{2,18},{10... | collective-permute-start | bytes 1179656 | tf_op jit(solution)/shard_map/ppermute | solution.py:29
  53.0 37.2 %collective-permute-start.14 = (bf16[16,64,768]{2,1,0:T(8,128)(2,1)}, bf16[16,64,768]{2,1,0:T(8,128)(2,1)}, u32[]{:S(2)}, u32[]{:S(2)}) collective-permute-start(bf16[16,64,768]{2,1,0:T(8,128)(2,1)} %constant_dynamic-update-slice_fusion.7.refs_4_.refs_10_), channel_id=1, source_target_pairs={{0,96},{32,0},{64,32},{96,64},{1,97},{33,1},{65,33},{97,65},{2,98}... | collective-permute-start | bytes 4718600 | tf_op jit(solution)/shard_map/ppermute | solution.py:29
  59.3 33.7 %collective-permute-start.7 = (bf16[16,64,768]{2,1,0:T(8,128)(2,1)}, bf16[16,64,768]{2,1,0:T(8,128)(2,1)}, u32[]{:S(2)}, u32[]{:S(2)}) collective-permute-start(bf16[16,64,768]{2,1,0:T(8,128)(2,1)} %constant_dynamic-update-slice_fusion.refs_2_.refs_8_), channel_id=1, source_target_pairs={{0,32},{32,64},{64,96},{96,0},{1,33},{33,65},{65,97},{97,1},{2,34}... | collective-permute-start | bytes 4718600 | tf_op jit(solution)/shard_map/ppermute | solution.py:29
  119.6 91.8 %collective-permute-start.15 = (bf16[2,1024,1024]{2,1,0:T(8,128)(2,1)}, bf16[2,1024,1024]{2,1,0:T(8,128)(2,1)}, u32[]{:S(2)}, u32[]{:S(2)}) collective-permute-start(bf16[2,1024,1024]{2,1,0:T(8,128)(2,1)} %shard_map.138.refs_3_), channel_id=1, source_target_pairs={{0,1},{1,0},{2,3},{3,2},{4,5},{5,4},{6,7},{7,6},{8,9},{9,8},{10,11... | collective-permute-start | bytes 12582920 | tf_op jit(solution)/shard_map/ppermute | solution.py:29
  133.5 13.5 %collective-permute-start.19 = (bf16[2,64,1024]{2,1,0:T(8,128)(2,1)S(1)}, bf16[2,64,1024]{2,1,0:T(8,128)(2,1)S(1)}, u32[]{:S(2)}, u32[]{:S(2)}) collective-permute-start(bf16[2,64,1024]{2,1,0:T(8,128)(2,1)S(1)} %get-tuple-element.18), channel_id=1, source_target_pairs={{0,24},{8,0},{16,8},{24,16},{1,25},{9,1},{17,9},{25,17},{2,26},{10... | collective-permute-start | bytes 786440 | tf_op jit(solution)/shard_map/ppermute | solution.py:29
  137.8 14.0 %collective-permute-start.24 = (bf16[2,64,1024]{2,1,0:T(8,128)(2,1)S(1)}, bf16[2,64,1024]{2,1,0:T(8,128)(2,1)S(1)}, u32[]{:S(2)}, u32[]{:S(2)}) collective-permute-start(bf16[2,64,1024]{2,1,0:T(8,128)(2,1)S(1)} %get-tuple-element.17), channel_id=1, source_target_pairs={{0,2},{2,4},{4,6},{6,0},{1,3},{3,5},{5,7},{7,1},{8,10},{10,12},{12... | collective-permute-start | bytes 786440 | tf_op jit(solution)/shard_map/ppermute | solution.py:29
  149.1 31.6 %collective-permute-start.21 = (bf16[8,64,1024]{2,1,0:T(8,128)(2,1)S(1)}, bf16[8,64,1024]{2,1,0:T(8,128)(2,1)S(1)}, u32[]{:S(2)}, u32[]{:S(2)}) collective-permute-start(bf16[8,64,1024]{2,1,0:T(8,128)(2,1)S(1)} %pad_maximum_fusion.refs_6_), channel_id=1, source_target_pairs={{0,2},{2,4},{4,6},{6,0},{1,3},{3,5},{5,7},{7,1},{8,10},{10,12},{12... | collective-permute-start | bytes 3145736 | tf_op jit(solution)/shard_map/ppermute | solution.py:29
  149.1 33.9 %collective-permute-start.22 = (bf16[8,64,1024]{2,1,0:T(8,128)(2,1)S(1)}, bf16[8,64,1024]{2,1,0:T(8,128)(2,1)S(1)}, u32[]{:S(2)}, u32[]{:S(2)}) collective-permute-start(bf16[8,64,1024]{2,1,0:T(8,128)(2,1)S(1)} %pad_maximum_fusion.refs_6_), channel_id=1, source_target_pairs={{0,6},{2,0},{4,2},{6,4},{1,7},{3,1},{5,3},{7,5},{8,14},{10,8},{12,... | collective-permute-start | bytes 3145736 | tf_op jit(solution)/shard_map/ppermute | solution.py:29
  151.8 26.7 %collective-permute-start.25 = (bf16[2,64,1024]{2,1,0:T(8,128)(2,1)S(1)}, bf16[2,64,1024]{2,1,0:T(8,128)(2,1)S(1)}, u32[]{:S(2)}, u32[]{:S(2)}) collective-permute-start(bf16[2,64,1024]{2,1,0:T(8,128)(2,1)S(1)} %get-tuple-element.17), channel_id=1, source_target_pairs={{0,6},{2,0},{4,2},{6,4},{1,7},{3,1},{5,3},{7,5},{8,14},{10,8},{12,... | collective-permute-start | bytes 786440 | tf_op jit(solution)/shard_map/ppermute | solution.py:29
  151.8 28.3 %collective-permute-start.26 = (bf16[2,64,1024]{2,1,0:T(8,128)(2,1)S(1)}, bf16[2,64,1024]{2,1,0:T(8,128)(2,1)S(1)}, u32[]{:S(2)}, u32[]{:S(2)}) collective-permute-start(bf16[2,64,1024]{2,1,0:T(8,128)(2,1)S(1)} %get-tuple-element.17), channel_id=1, source_target_pairs={{0,4},{2,6},{4,0},{6,2},{1,5},{3,7},{5,1},{7,3},{8,12},{10,14},{12... | collective-permute-start | bytes 786440 | tf_op jit(solution)/shard_map/ppermute | solution.py:29
  178.6 15.3 %collective-permute-start.23 = (bf16[8,64,1024]{2,1,0:T(8,128)(2,1)S(1)}, bf16[8,64,1024]{2,1,0:T(8,128)(2,1)}, u32[]{:S(2)}, u32[]{:S(2)}) collective-permute-start(bf16[8,64,1024]{2,1,0:T(8,128)(2,1)S(1)} %pad_maximum_fusion.refs_6_), channel_id=1, source_target_pairs={{0,4},{2,6},{4,0},{6,2},{1,5},{3,7},{5,1},{7,3},{8,12},{10,14},{12... | collective-permute-start | bytes 3145736 | tf_op jit(solution)/shard_map/ppermute | solution.py:29
  180.3 15.0 %collective-permute-start.27 = (bf16[8,64,1024]{2,1,0:T(8,128)(2,1)S(1)}, bf16[8,64,1024]{2,1,0:T(8,128)(2,1)}, u32[]{:S(2)}, u32[]{:S(2)}) collective-permute-start(bf16[8,64,1024]{2,1,0:T(8,128)(2,1)S(1)} %pad_maximum_fusion.1.refs_10_), channel_id=1, source_target_pairs={{0,8},{8,16},{16,24},{24,0},{1,9},{9,17},{17,25},{25,1},{2,10},{10... | collective-permute-start | bytes 3145736 | tf_op jit(solution)/shard_map/ppermute | solution.py:29
  180.7 23.4 %collective-permute-start.28 = (bf16[8,64,1024]{2,1,0:T(8,128)(2,1)S(1)}, bf16[8,64,1024]{2,1,0:T(8,128)(2,1)}, u32[]{:S(2)}, u32[]{:S(2)}) collective-permute-start(bf16[8,64,1024]{2,1,0:T(8,128)(2,1)S(1)} %pad_maximum_fusion.1.refs_10_), channel_id=1, source_target_pairs={{0,24},{8,0},{16,8},{24,16},{1,25},{9,1},{17,9},{25,17},{2,26},{10... | collective-permute-start | bytes 3145736 | tf_op jit(solution)/shard_map/ppermute | solution.py:29
  184.0 27.4 %collective-permute-start.29 = (bf16[8,64,1024]{2,1,0:T(8,128)(2,1)S(1)}, bf16[8,64,1024]{2,1,0:T(8,128)(2,1)}, u32[]{:S(2)}, u32[]{:S(2)}) collective-permute-start(bf16[8,64,1024]{2,1,0:T(8,128)(2,1)S(1)} %pad_maximum_fusion.1.refs_10_), channel_id=1, source_target_pairs={{0,16},{8,24},{16,0},{24,8},{1,17},{9,25},{17,1},{25,9},{2,18},{10... | collective-permute-start | bytes 3145736 | tf_op jit(solution)/shard_map/ppermute | solution.py:29
  193.8 66.5 %collective-permute-start.31 = (bf16[8,64,2048]{2,1,0:T(8,128)(2,1)}, bf16[8,64,2048]{2,1,0:T(8,128)(2,1)}, u32[]{:S(2)}, u32[]{:S(2)}) collective-permute-start(bf16[8,64,2048]{2,1,0:T(8,128)(2,1)} %bitcast.14), channel_id=1, source_target_pairs={{0,32},{32,64},{64,96},{96,0},{1,33},{33,65},{65,97},{97,1},{2,34}... | collective-permute-start | bytes 6291464 | tf_op jit(solution)/shard_map/ppermute | solution.py:29
  195.3 65.0 %collective-permute-start.32 = (bf16[8,64,2048]{2,1,0:T(8,128)(2,1)}, bf16[8,64,2048]{2,1,0:T(8,128)(2,1)}, u32[]{:S(2)}, u32[]{:S(2)}) collective-permute-start(bf16[8,64,2048]{2,1,0:T(8,128)(2,1)} %bitcast.15), channel_id=1, source_target_pairs={{0,96},{32,0},{64,32},{96,64},{1,97},{33,1},{65,33},{97,65},{2,98}... | collective-permute-start | bytes 6291464 | tf_op jit(solution)/shard_map/ppermute | solution.py:29
  241.9 28.3 %collective-permute-start.30 = (bf16[1024,1024]{1,0:T(8,128)(2,1)}, bf16[1024,1024]{1,0:T(8,128)(2,1)S(1)}, u32[]{:S(2)}, u32[]{:S(2)}) collective-permute-start(bf16[1024,1024]{1,0:T(8,128)(2,1)} %shard_map.140.mine_a), channel_id=1, source_target_pairs={{0,1},{1,0},{2,3},{3,2},{4,5},{5,4},{6,7},{7,6},{8,9},{9,8},{10,11... | collective-permute-start | bytes 6291464 | tf_op jit(solution)/shard_map/ppermute | solution.py:29
  (23 other events, 237.1 us)
Sparse Core Ops, SparseCore 0:
  24.5 59.8 all-gather.2
where the time goes:
time: 293 us; the launch traced here: 290 us
  waiting for transfers between devices  108 us (37%)
  Pallas kernels  80 us (27%)
  starting transfers between devices  63.5 us (22%)
  local copies, waits for them, and re-layouts  19.5 us (7%)
  between operations  13.6 us (5%)
  other arithmetic  4.95 us (2%)
    ppermute x34, waiting for transfers between devices, step(): return lax.ppermute(v, over, [(i, (i + shift) % size) for i in range(size)])  108 us
    ppermute x34, starting transfers between devices, step(): return lax.ppermute(v, over, [(i, (i + shift) % size) for i in range(size)])  63.5 us
    pallas_call x1, Pallas kernels, local(): call(functools.partial(ffn_kernel, la + lb), (whole, shape((length, hidde...  20.7 us
    pallas_call x2, Pallas kernels, turned(): call(functools.partial(turned_kernel, layout, plane), one_half, [SMEM, HB...  19.4 us
    pallas_call x1, Pallas kernels, local(): call(functools.partial(mixer_kernel, la + lb), partial, [SMEM] + [VMEM] *...  16.7 us
    unnamed x36, local copies, waits for them, and re-layouts  10.6 us
    pallas_call x1, Pallas kernels, local(): call(functools.partial(project_kernel, la + lb), (some, some), [SMEM, VME...  9.89 us
    pallas_call x1, Pallas kernels, local(): call(closing_kernel, one_half, [SMEM] + [HBM] * 5 + [VMEM], 2000000000.0,...  7.19 us
  transfers between devices with their start and end apart: 35, of which 17 were waited for; matrix products, arithmetic and copies ran while one was open for 7% of the time, Pallas kernels for 25%

commit v1 on v0

--- a/solution.py
+++ b/solution.py
@@ -98,32 +98,23 @@
     lax.fori_loop(0, own.shape[0] // TILE, rows, 0)
 
 
-def project_kernel(layout, *refs):
-    n = len(layout)
-    pos, normed = refs[:2]
-    pieces, (gate, inner) = refs[2 : 2 + n], refs[2 + n : 4 + n]
-    weights, sem = refs[4 + n :]
+def mixer_kernel(in_layout, out_layout, *refs):
+    n, m = len(in_layout), len(out_layout)
+    pos, normed, taps, recur_gate, inlet_gate, rate, shift = refs[:7]
+    in_pieces, out_pieces, part_out = refs[7 : 7 + n], refs[7 + n : 7 + n + m], refs[7 + n + m]
+    entry, gate, padded, decay, drive, prod, weights, part = refs[8 + n + m : -3]
+    in_sem, weight_sem, out_sem = refs[-3:]
     length, channels = gate.shape
-    start_weights(pieces, layout, pos, weights, sem)
-    pltpu.make_async_copy(weights, weights, sem).wait()
-    for r in range(0, length, TILE):
-        x = normed[r : r + TILE, :]
-        both = jnp.dot(x, weights[...], preferred_element_type=f32).astype(bf16)
-        gate[r : r + TILE, :] = both[:, :channels]
-        inner[r : r + TILE, :] = both[:, channels:]
-
-
-def mixer_kernel(layout, *refs):
-    n = len(layout)
-    pos, gate, inner, taps, recur_gate, inlet_gate, rate, shift = refs[:8]
-    pieces, part_out = refs[8 : 8 + n], refs[8 + n]
-    padded, decay, drive, prod, weights, part, weight_sem, out_sem = refs[9 + n :]
-    length, channels = gate.shape
-    start_weights(pieces, layout, pos, weights, weight_sem)
+    start_weights(in_pieces, in_layout, pos, entry, in_sem)
+    start_weights(out_pieces, out_layout, pos, weights, weight_sem)
     padded[:8, :] = jnp.zeros((8, channels), f32)
     blocks, block = recur_gate.shape[0], recur_gate.shape[1]
+    pltpu.make_async_copy(entry, entry, in_sem).wait()
     for r in range(0, length, TILE):
-        padded[8 + r : 8 + r + TILE, :] = inner[r : r + TILE, :].astype(f32)
+        both = jnp.dot(normed[r : r + TILE, :], entry[...], preferred_element_type=f32)
+        both = both.astype(bf16)
+        gate[r : r + TILE, :] = both[:, :channels]
+        padded[8 + r : 8 + r + TILE, :] = both[:, channels:].astype(f32)
         acc = padded[r + 5 : r + 5 + TILE, :] * taps[0:1, :]
         for k in range(1, 4):
             acc = acc + padded[r + 5 + k : r + 5 + k + TILE, :] * taps[k : k + 1, :]
@@ -226,15 +217,18 @@
     return lax.dot_general(left, right, (((1,), (1,)), ((), ())), preferred_element_type=f32)
 
 
-def ffn_kernel(layout, *refs):
+def ffn_kernel(layout, down_layout, *refs):
     pos, own, other, mine, theirs, gain = refs[:6]
-    n = len(layout)
-    pieces, (mid_out, act_out) = refs[6 : 6 + n], refs[6 + n : 8 + n]
-    stream, parts, up, normed, mid, act, up_sem, in_sem, out_sem, mid_sem = refs[8 + n :]
+    n, m = len(layout), len(down_layout)
+    pieces, down_pieces = refs[6 : 6 + n], refs[6 + n : 6 + n + m]
+    mid_out, act_out, part_out = refs[6 + n + m : 9 + n + m]
+    stream, parts, up, down, mid, act, part = refs[9 + n + m : 16 + n + m]
     tiles = own.shape[0] // TILE
+    normed = refs[16 + n + m : 16 + n + m + tiles]
+    up_sem, down_sem, in_sem, act_sem, mid_sem, part_sem = refs[16 + n + m + tiles :]
 
     def arriving(t):
-        s = pl.ds(pl.multiple_of(t * TILE, TILE), TILE)
+        s = slice(t * TILE, (t + 1) * TILE)
         pairs = [
             (own, stream.at[0]),
             (other, stream.at[1]),
@@ -249,7 +243,9 @@
         ]
 
     def norm(t):
-        s = pl.ds(pl.multiple_of(t * TILE, TILE), TILE)
+        for c in arriving(t):
+            c.wait()
+        s = slice(t * TILE, (t + 1) * TILE)
         halves = []
         for h in range(2):
             v = stream[h, s, :].astype(f32) + (
@@ -261,43 +257,36 @@
         a, b = halves
         ms = (jnp.sum(a * a, -1, keepdims=True) + jnp.sum(b * b, -1, keepdims=True)) / D
         r = lax.rsqrt(ms + epsilon)
-        normed[s, :HALF] = (a * r * gain[:, :HALF]).astype(bf16)
-        normed[s, HALF:] = (b * r * gain[:, HALF:]).astype(bf16)
+        normed[t][:, :HALF] = (a * r * gain[:, :HALF]).astype(bf16)
+        normed[t][:, HALF:] = (b * r * gain[:, HALF:]).astype(bf16)
+        pltpu.make_async_copy(mid.at[s, :], mid_out.at[s, :], mid_sem).start()
 
     for c in arriving(0):
         c.start()
     start_weights(pieces, layout, pos, up, up_sem)
-    for t in range(1, tiles):
+    for c in arriving(1):
+        c.start()
+    start_weights(down_pieces, down_layout, pos, down, down_sem, 0)
+    for t in range(2, tiles):
         for c in arriving(t):
             c.start()
-    for c in arriving(0):
-        c.wait()
     norm(0)
     pltpu.make_async_copy(up, up, up_sem).wait()
-
-    def product(t):
-        s = pl.ds(pl.multiple_of(t * TILE, TILE), TILE)
-        prod = jnp.dot(normed[s, :], up[...], preferred_element_type=f32)
-        act[s, :] = jnp.square(jnp.maximum(prod, 0.0)).astype(bf16)
-
-    def leave(t):
-        s = pl.ds(pl.multiple_of(t * TILE, TILE), TILE)
-        pltpu.make_async_copy(mid.at[s, :], mid_out.at[s, :], mid_sem).start()
-        pltpu.make_async_copy(act.at[s, :], act_out.at[s, :], out_sem).start()
-
-    def rows(t, _):
-        for c in arriving(t + 1):
-            c.wait()
-        norm(t + 1)
-        product(t)
-        leave(t)
-        return 0
-
-    lax.fori_loop(0, tiles - 1, rows, 0)
-    product(tiles - 1)
-    leave(tiles - 1)
+    for t in range(tiles):
+        s = slice(t * TILE, (t + 1) * TILE)
+        if t + 1 < tiles:
+            norm(t + 1)
+        prod = jnp.dot(normed[t][...], up[...], preferred_element_type=f32)
+        left = jnp.square(jnp.maximum(prod, 0.0)).astype(bf16)
+        act[s, :] = left
+        pltpu.make_async_copy(act.at[s, :], act_out.at[s, :], act_sem).start()
+        if t == 0:
+            pltpu.make_async_copy(down, down, down_sem).wait()
+        part[s, :] = dot_turned(left, down[...]).astype(bf16)
+        pltpu.make_async_copy(part.at[s, :], part_out.at[s, :], part_sem).start()
     pltpu.make_async_copy(mid, mid_out, mid_sem).wait()
-    pltpu.make_async_copy(act, act_out, out_sem).wait()
+    pltpu.make_async_copy(act, act_out, act_sem).wait()
+    pltpu.make_async_copy(part, part_out, part_sem).wait()
 
 
 def closing_kernel(pos, mid, mine_a, theirs_a, mine_b, theirs_b, gain, out_ref, *scratch):
@@ -308,15 +297,14 @@
     def arriving(t):
         s = slice(t * TILE, (t + 1) * TILE)
         pairs = [
-            (mid, stream),
-            (mine_a, parts.at[near, 0]),
-            (theirs_a, parts.at[near, 1]),
-            (mine_b, parts.at[1 - near, 0]),
-            (theirs_b, parts.at[1 - near, 1]),
+            (mid.at[s, :HALF], stream.at[near, s, :]),
+            (mid.at[s, HALF:], stream.at[1 - near, s, :]),
+            (mine_a.at[s, :], parts.at[0, s, :]),
+            (theirs_a.at[s, :], parts.at[1, s, :]),
+            (mine_b.at[s, :], parts.at[2, s, :]),
         ]
         return [
-            pltpu.make_async_copy(src.at[s, :], dst.at[s, :], in_sem.at[t, k])
-            for k, (src, dst) in enumerate(pairs)
+            pltpu.make_async_copy(src, dst, in_sem.at[t, k]) for k, (src, dst) in enumerate(pairs)
         ]
 
     for t in range(tiles):
@@ -327,13 +315,15 @@
             c.wait()
         for half in range(2):
             s = slice(t * TILE + half * 128, t * TILE + half * 128 + 128)
-            a, b = [
-                stream[s, h * HALF : h * HALF + HALF].astype(f32)
-                + (parts[h, 0, s, :].astype(f32) + parts[h, 1, s, :].astype(f32))
-                for h in range(2)
-            ]
+            a = stream[0, s, :].astype(f32) + (
+                parts[0, s, :].astype(f32) + parts[1, s, :].astype(f32)
+            )
+            b = stream[1, s, :].astype(f32) + (
+                parts[2, s, :].astype(f32) + theirs_b[s, :].astype(f32)
+            )
             ms = (jnp.sum(a * a, -1, keepdims=True) + jnp.sum(b * b, -1, keepdims=True)) / D
-            out[s, :] = (a * lax.rsqrt(ms + epsilon) * gain[...]).astype(bf16)
+            mine = jnp.where(near == 0, a, b)
+            out[s, :] = (mine * lax.rsqrt(ms + epsilon) * gain[...]).astype(bf16)
         s = slice(t * TILE, (t + 1) * TILE)
         pltpu.make_async_copy(out.at[s, :], out_ref.at[s, :], out_sem).start()
     pltpu.make_async_copy(out, out_ref, out_sem).wait()
@@ -343,7 +333,7 @@
     return pl.CostEstimate(flops=int(flops), bytes_accessed=int(moved_bytes), transcendentals=0)
 
 
-def call(kernel, out_shapes, specs, flops, scratch=(), outs=VMEM):
+def call(kernel, out_shapes, specs, flops, scratch=(), outs=VMEM, room=56):
     return pl.pallas_call(
         kernel,
         out_shape=out_shapes,
@@ -351,7 +341,7 @@
         out_specs=jax.tree.map(lambda _: outs, out_shapes),
         scratch_shapes=list(scratch),
         cost_estimate=cost(flops, 8e6),
-        compiler_params=pltpu.CompilerParams(vmem_limit_bytes=56 * 2**20),
+        compiler_params=pltpu.CompilerParams(vmem_limit_bytes=room * 2**20),
     )
 
 
@@ -410,34 +400,27 @@
     up_x = ring_pieces(*later, "x")
     later = whole_ring(pair[:, :, mid_col:], places, "x")
     up_y = ring_pieces(*later, "y")
-    down_t = lax.optimization_barrier((down_t, by_x[0], by_y[0]))[0]
     plane = lax.all_gather(down_t, ("y", "x"), axis=0, tiled=False)
     down_pieces = plane_pieces(plane, 0, hidden)
 
     shape = jax.ShapeDtypeStruct
     whole, one_half = shape((length, D), bf16), shape((length, HALF), bf16)
-    normed = call(norm_kernel, whole, [VMEM] * 3, 2e9)(own, other, own_first(mixer_gain))
-
+    normed = call(norm_kernel, whole, [VMEM] * 3, 2e9, room=24)(own, other, own_first(mixer_gain))
+
+    scan_buffer = pltpu.VMEM((channels // 128, length, 128), f32)
     a, la = flat(x_pieces, 0, channels)
     b, lb = flat(y_pieces, channels, channels, part)
-    some = shape((length, channels), bf16)
-    gate, inner = call(
-        functools.partial(project_kernel, la + lb),
-        (some, some),
-        [SMEM, VMEM] + [HBM] * len(la + lb),
-        4 * length * channels * D,
-        [pltpu.VMEM((D, 2 * channels), bf16), pltpu.SemaphoreType.DMA],
-    )(pos, normed, *a, *b)
-    scan_buffer = pltpu.VMEM((channels // 128, length, 128), f32)
-    a, la = flat(x_pieces, 0, part, channels)
-    b, lb = flat(y_pieces, part, part)
+    c, lc = flat(x_pieces, 0, part, channels)
+    d, ld = flat(y_pieces, part, part)
     partial = shape((2, length, HALF), bf16)
     mine = call(
-        functools.partial(mixer_kernel, la + lb),
+        functools.partial(mixer_kernel, la + lb, lc + ld),
         partial,
-        [SMEM] + [VMEM] * 7 + [HBM] * len(la + lb),
+        [SMEM] + [VMEM] * 6 + [HBM] * len(la + lb + lc + ld),
         1.2e10,
         [
+            pltpu.VMEM((D, 2 * channels), bf16),
+            pltpu.VMEM((length, channels), bf16),
             pltpu.VMEM((length + 8, channels), f32),
             scan_buffer,
             scan_buffer,
@@ -446,12 +429,12 @@
             pltpu.VMEM((2, length, HALF), bf16),
             pltpu.SemaphoreType.DMA,
             pltpu.SemaphoreType.DMA,
+            pltpu.SemaphoreType.DMA,
         ],
         HBM,
     )(
         pos,
-        gate,
-        inner,
+        normed,
         filter_taps,
         recur_gate,
         inlet_gate,
@@ -459,6 +442,8 @@
         decay_shift.reshape(length, 1),
         *a,
         *b,
+        *c,
+        *d,
     )
     theirs = step(mine, "tp", 1)
     tiles = length // TILE
@@ -483,42 +468,49 @@
 
     a, la = flat(up_x, 0, mid_col)
     b, lb = flat(up_y, mid_col, mid_col)
-    mid, activated = call(
-        functools.partial(ffn_kernel, la + lb),
-        (whole, shape((length, hidden), bf16)),
-        [SMEM] + [HBM] * 4 + [VMEM] + [HBM] * len(la + lb),
-        2 * length * hidden * D,
+    c, lc = flat(down_pieces[:1], 0, hidden)
+    mid, activated, mine_c = call(
+        functools.partial(ffn_kernel, la + lb, lc),
+        (whole, shape((length, hidden), bf16), one_half),
+        [SMEM] + [HBM] * 4 + [VMEM] + [HBM] * len(la + lb + lc),
+        3 * length * hidden * D,
         [
             pltpu.VMEM((2, length, HALF), bf16),
             pltpu.VMEM((2, 2, length, HALF), bf16),
             pltpu.VMEM((D, hidden), bf16),
-            pltpu.VMEM((length, D), bf16),
+            pltpu.VMEM((HALF, hidden), bf16),
             pltpu.VMEM((length, D), bf16),
             pltpu.VMEM((length, hidden), bf16),
+            pltpu.VMEM((length, HALF), bf16),
+        ]
+        + [pltpu.VMEM((TILE, D), bf16)] * tiles
+        + [
+            pltpu.SemaphoreType.DMA,
             pltpu.SemaphoreType.DMA,
             pltpu.SemaphoreType.DMA((tiles, 6)),
+            pltpu.SemaphoreType.DMA,
             pltpu.SemaphoreType.DMA,
             pltpu.SemaphoreType.DMA,
         ],
         HBM,
-    )(pos, own, other, mine, theirs, own_first(feedforward_gain), *a, *b)
-    mine_c = turned(activated, down_pieces[:1], 0)
+    )(pos, own, other, mine, theirs, own_first(feedforward_gain), *a, *b, *c)
     theirs_c = step(mine_c, "tp", 1)
     mine_d = turned(activated, down_pieces[1:], 1)
     theirs_d = step(mine_d, "tp", 1)
     out = call(
         closing_kernel,
         one_half,
-        [SMEM] + [HBM] * 5 + [VMEM],
+        [SMEM] + [HBM] * 4 + [VMEM] * 2,
         2e9,
         [
-            pltpu.VMEM((length, D), bf16),
-            pltpu.VMEM((2, 2, length, HALF), bf16),
+            pltpu.VMEM((2, length, HALF), bf16),
+            pltpu.VMEM((3, length, HALF), bf16),
             pltpu.VMEM((length, HALF), bf16),
             pltpu.SemaphoreType.DMA((tiles, 5)),
             pltpu.SemaphoreType.DMA,
         ],
         HBM,
+        24,
     )(pos, mid, mine_c, theirs_c, mine_d, theirs_d, final_gain.reshape(1, HALF))
     return out.reshape(num_seq, length, half)
 

time: 293 us -> 311 us (1.061)
  the two profiles are of different devices: /device:TPU:1 before, /device:TPU:19 now
where the time goes in v1:
time: 311 us; the launch traced here: 306 us
  starting transfers between devices  112 us (36%)
  waiting for transfers between devices  84.5 us (27%)
  Pallas kernels  68.6 us (22%)
  local copies, waits for them, and re-layouts  21.3 us (7%)
  between operations  13.9 us (4%)
  other arithmetic  5.93 us (2%)
    ppermute x34, starting transfers between devices, step(): return lax.ppermute(v, over, [(i, (i + shift) % size) for i in range(size)])  112 us
    ppermute x34, waiting for transfers between devices, step(): return lax.ppermute(v, over, [(i, (i + shift) % size) for i in range(size)])  83.8 us
    pallas_call x1, Pallas kernels, local(): call(functools.partial(ffn_kernel, la + lb, lc), (whole, shape((length, h...  25.6 us
    pallas_call x1, Pallas kernels, local(): call(functools.partial(mixer_kernel, la + lb, lc + ld), partial, [SMEM] +...  24.4 us
    unnamed x42, local copies, waits for them, and re-layouts  13.2 us
    pallas_call x1, Pallas kernels, turned(): call(functools.partial(turned_kernel, layout, plane), one_half, [SMEM, HB...  10.2 us
  transfers between devices with their start and end apart: 35, of which 11 were waited for; matrix products, arithmetic and copies ran while one was open for 7% of the time, Pallas kernels for 21%

profile of v1, /device:TPU:19, one launch (start us, length us, event | category | flops | bytes accessed | tf_op | source)
XLA Modules:
  0.0 306.5 jit_solution(813354743788862794)
XLA Ops:
  27.7 6.6 %collective-permute-done.11 = bf16[4,64,768]{2,1,0:T(8,128)(2,1)S(1)} collective-permute-done((bf16[4,64,768]{2,1,0:T(8,128)(2,1)S(1)}, bf16[4,64,768]{2,1,0:T(8,128)(2,1)S(1)}, u32[]{:S(2)}, u32[]{:S(2)}) %collective-permute-start.11) | collective-permute-done | bytes 393248 | tf_op jit(solution)/shard_map/ppermute | solution.py:29
  39.5 4.3 %collective-permute-done.13 = bf16[4,64,768]{2,1,0:T(8,128)(2,1)S(1)} collective-permute-done((bf16[4,64,768]{2,1,0:T(8,128)(2,1)S(1)}, bf16[4,64,768]{2,1,0:T(8,128)(2,1)S(1)}, u32[]{:S(2)}, u32[]{:S(2)}) %collective-permute-start.13) | collective-permute-done | bytes 393248 | tf_op jit(solution)/shard_map/ppermute | solution.py:29
  44.6 3.8 %collective-permute-start.14 = (bf16[16,64,768]{2,1,0:T(8,128)(2,1)}, bf16[16,64,768]{2,1,0:T(8,128)(2,1)}, u32[]{:S(2)}, u32[]{:S(2)}) collective-permute-start(bf16[16,64,768]{2,1,0:T(8,128)(2,1)} %constant_dynamic-update-slice_fusion.7.refs_9_.refs_13_), channel_id=1, source_target_pairs={{0,96},{32,0},{64,32},{96,64},{1,97},{33,1},{65,33},{97,65},{2,98}... | collective-permute-start | bytes 4718600 | tf_op jit(solution)/shard_map/ppermute | solution.py:29
  53.6 3.2 %shard_map.136.refs_1_ = bf16[1024,2048]{1,0:T(8,128)(2,1)S(1)} custom-call(bf16[1024,1024]{1,0:T(8,128)(2,1)S(1)} %bitcast.35, bf16[1024,1024]{1,0:T(8,128)(2,1)} %collective-permute-done.other.refs_2_, f32[1,2048]{1,0:T(1,128)S(1)} %bitcast.36), custom_call_target="tpu_custom_call" | custom-call | flops 2000000000 | bytes 8000000 | tf_op jit(solution)/shard_map/pallas_call | solution.py:408
  58.8 22.7 %collective-permute-done.14.refs_10_.refs_14_ = bf16[16,64,768]{2,1,0:T(8,128)(2,1)} collective-permute-done((bf16[16,64,768]{2,1,0:T(8,128)(2,1)}, bf16[16,64,768]{2,1,0:T(8,128)(2,1)}, u32[]{:S(2)}, u32[]{:S(2)}) %collective-permute-start.14) | collective-permute-done | bytes 1572896 | tf_op jit(solution)/shard_map/ppermute | solution.py:29
  81.5 24.4 %shard_map.137.refs_3_ = bf16[2,1024,1024]{2,1,0:T(8,128)(2,1)} custom-call(s32[4]{0:T(128)} %pad_add_fusion.refs_0_.pos, bf16[1024,2048]{1,0:T(8,128)(2,1)} %copy-done.1, f32[4,512]{1,0:T(4,128)} %refs_2_.1, bf16[2,256,256]{2,1,0:T(8,128)(2,1)} %refs_3_.1, bf16[2,256,256]{2,1,0:T(8,128)(2,1)} %refs_4_.1, f32[1,512]{1,0:T(1,128)} %bitcast.45, ...), custom_call_target="tpu_custom_call" | custom-call | flops 12000000000 | bytes 8000000 | tf_op jit(solution)/shard_map/pallas_call | solution.py:416
  105.9 7.8 %collective-permute-start.15 = (bf16[2,1024,1024]{2,1,0:T(8,128)(2,1)}, bf16[2,1024,1024]{2,1,0:T(8,128)(2,1)}, u32[]{:S(2)}, u32[]{:S(2)}) collective-permute-start(bf16[2,1024,1024]{2,1,0:T(8,128)(2,1)} %shard_map.137.refs_3_), channel_id=1, source_target_pairs={{0,1},{1,0},{2,3},{3,2},{4,5},{5,4},{6,7},{7,6},{8,9},{9,8},{10,11... | collective-permute-start | bytes 12582920 | tf_op jit(solution)/shard_map/ppermute | solution.py:29
  113.8 3.2 %collective-permute-start.17 = (bf16[32,2048]{1,0:T(8,128)(2,1)S(1)}, bf16[32,2048]{1,0:T(8,128)(2,1)S(1)}, u32[]{:S(2)}, u32[]{:S(2)}) collective-permute-start(bf16[32,2048]{1,0:T(8,128)(2,1)S(1)} %get-tuple-element.16), channel_id=1, source_target_pairs={{0,96},{32,0},{64,32},{96,64},{1,97},{33,1},{65,33},{97,65},{2,98}... | collective-permute-start | bytes 393224 | tf_op jit(solution)/shard_map/ppermute | solution.py:29
  117.0 3.0 collective-permute-done.16
  120.1 13.6 %collective-permute-start.18 = (bf16[2,64,1024]{2,1,0:T(8,128)(2,1)S(1)}, bf16[2,64,1024]{2,1,0:T(8,128)(2,1)S(1)}, u32[]{:S(2)}, u32[]{:S(2)}) collective-permute-start(bf16[2,64,1024]{2,1,0:T(8,128)(2,1)S(1)} %get-tuple-element.14), channel_id=1, source_target_pairs={{0,8},{8,16},{16,24},{24,0},{1,9},{9,17},{17,25},{25,1},{2,10},{10... | collective-permute-start | bytes 786440 | tf_op jit(solution)/shard_map/ppermute | solution.py:29
  135.6 7.2 %collective-permute-start.24 = (bf16[2,64,1024]{2,1,0:T(8,128)(2,1)S(1)}, bf16[2,64,1024]{2,1,0:T(8,128)(2,1)S(1)}, u32[]{:S(2)}, u32[]{:S(2)}) collective-permute-start(bf16[2,64,1024]{2,1,0:T(8,128)(2,1)S(1)} %get-tuple-element.13), channel_id=1, source_target_pairs={{0,2},{2,4},{4,6},{6,0},{1,3},{3,5},{5,7},{7,1},{8,10},{10,12},{12... | collective-permute-start | bytes 786440 | tf_op jit(solution)/shard_map/ppermute | solution.py:29
  144.2 7.3 %collective-permute-start.21 = (bf16[8,64,1024]{2,1,0:T(8,128)(2,1)S(1)}, bf16[8,64,1024]{2,1,0:T(8,128)(2,1)S(1)}, u32[]{:S(2)}, u32[]{:S(2)}) collective-permute-start(bf16[8,64,1024]{2,1,0:T(8,128)(2,1)S(1)} %pad_maximum_fusion.refs_6_), channel_id=1, source_target_pairs={{0,2},{2,4},{4,6},{6,0},{1,3},{3,5},{5,7},{7,1},{8,10},{10,12},{12... | collective-permute-start | bytes 3145736 | tf_op jit(solution)/shard_map/ppermute | solution.py:29
  151.5 13.0 %collective-permute-start.22 = (bf16[8,64,1024]{2,1,0:T(8,128)(2,1)S(1)}, bf16[8,64,1024]{2,1,0:T(8,128)(2,1)S(1)}, u32[]{:S(2)}, u32[]{:S(2)}) collective-permute-start(bf16[8,64,1024]{2,1,0:T(8,128)(2,1)S(1)} %pad_maximum_fusion.refs_6_), channel_id=1, source_target_pairs={{0,6},{2,0},{4,2},{6,4},{1,7},{3,1},{5,3},{7,5},{8,14},{10,8},{12,... | collective-permute-start | bytes 3145736 | tf_op jit(solution)/shard_map/ppermute | solution.py:29
  167.1 23.8 %collective-permute-done.25 = bf16[2,64,1024]{2,1,0:T(8,128)(2,1)S(1)} collective-permute-done((bf16[2,64,1024]{2,1,0:T(8,128)(2,1)S(1)}, bf16[2,64,1024]{2,1,0:T(8,128)(2,1)S(1)}, u32[]{:S(2)}, u32[]{:S(2)}) %collective-permute-start.25) | collective-permute-done | bytes 262176 | tf_op jit(solution)/shard_map/ppermute | solution.py:29
  190.9 6.0 %collective-permute-start.23 = (bf16[8,64,1024]{2,1,0:T(8,128)(2,1)S(1)}, bf16[8,64,1024]{2,1,0:T(8,128)(2,1)}, u32[]{:S(2)}, u32[]{:S(2)}) collective-permute-start(bf16[8,64,1024]{2,1,0:T(8,128)(2,1)S(1)} %pad_maximum_fusion.refs_6_), channel_id=1, source_target_pairs={{0,4},{2,6},{4,0},{6,2},{1,5},{3,7},{5,1},{7,3},{8,12},{10,14},{12... | collective-permute-start | bytes 3145736 | tf_op jit(solution)/shard_map/ppermute | solution.py:29
  204.4 4.1 %fusion.2 = (bf16[512,2048]{1,0:T(8,128)(2,1)S(1)}, bf16[512,2048]{1,0:T(8,128)(2,1)}) fusion(bf16[1024,2048]{1,0:T(8,128)(2,1)} %all-gather.3.cloned.1.call-done), kind=kLoop, calls=%fused_computation.30 | loop fusion | bytes 8388608 | tf_op jit(solution)/shard_map/slice | solution.py:66
  208.5 3.6 %collective-permute-done.23.refs_9_ = bf16[8,64,1024]{2,1,0:T(8,128)(2,1)} collective-permute-done((bf16[8,64,1024]{2,1,0:T(8,128)(2,1)S(1)}, bf16[8,64,1024]{2,1,0:T(8,128)(2,1)}, u32[]{:S(2)}, u32[]{:S(2)}) %collective-permute-start.23) | collective-permute-done | bytes 1048608 | tf_op jit(solution)/shard_map/ppermute | solution.py:29
  212.4 10.9 %collective-permute-done.27.refs_11_ = bf16[8,64,1024]{2,1,0:T(8,128)(2,1)} collective-permute-done((bf16[8,64,1024]{2,1,0:T(8,128)(2,1)}, bf16[8,64,1024]{2,1,0:T(8,128)(2,1)}, u32[]{:S(2)}, u32[]{:S(2)}) %collective-permute-start.27) | collective-permute-done | bytes 1048608 | tf_op jit(solution)/shard_map/ppermute | solution.py:29
  223.3 4.4 %collective-permute-start.32 = (bf16[8,64,2048]{2,1,0:T(8,128)(2,1)S(1)}, bf16[8,64,2048]{2,1,0:T(8,128)(2,1)}, u32[]{:S(2)}, u32[]{:S(2)}) collective-permute-start(bf16[8,64,2048]{2,1,0:T(8,128)(2,1)S(1)} %bitcast.39), channel_id=1, source_target_pairs={{0,96},{32,0},{64,32},{96,64},{1,97},{33,1},{65,33},{97,65},{2,98}... | collective-permute-start | bytes 6291464 | tf_op jit(solution)/shard_map/ppermute | solution.py:29
  229.8 25.6 %shard_map.138 = (bf16[1024,2048]{1,0:T(8,128)(2,1)}, bf16[1024,2048]{1,0:T(8,128)(2,1)}, bf16[1024,1024]{1,0:T(8,128)(2,1)}) custom-call(s32[4]{0:T(128)} %pad_add_fusion.refs_0_.pos, bf16[1024,1024]{1,0:T(8,128)(2,1)} %bitcast.34, bf16[1024,1024]{1,0:T(8,128)(2,1)} %collective-permute-done.other.refs_2_, bf16[2,1024,1024]{2,1,0:T(8,128)(2,1)} %shard_map.137.refs_3_, ...), custom_call_target="tpu_custom_call" | custom-call | flops 12884901888 | bytes 8000000 | tf_op jit(solution)/shard_map/pallas_call | solution.py:472
  255.4 22.4 %collective-permute-start.30 = (bf16[1024,1024]{1,0:T(8,128)(2,1)}, bf16[1024,1024]{1,0:T(8,128)(2,1)}, u32[]{:S(2)}, u32[]{:S(2)}) collective-permute-start(bf16[1024,1024]{1,0:T(8,128)(2,1)} %get-tuple-element.9.mine_a), channel_id=1, source_target_pairs={{0,1},{1,0},{2,3},{3,2},{4,5},{5,4},{6,7},{7,6},{8,9},{9,8},{10,11... | collective-permute-start | bytes 6291464 | tf_op jit(solution)/shard_map/ppermute | solution.py:29
  277.9 10.2 %shard_map.139.mine_b = bf16[1024,1024]{1,0:T(8,128)(2,1)} custom-call(s32[4]{0:T(128)} %pad_add_fusion.refs_0_.pos, bf16[1024,2048]{1,0:T(8,128)(2,1)} %get-tuple-element.10.refs_1_, bf16[8,64,2048]{2,1,0:T(8,128)(2,1)} %collective-permute-done.31.refs_2_, bf16[8,64,2048]{2,1,0:T(8,128)(2,1)} %collective-permute-done.32.refs_3_), custom_call_target="tpu_custom_call" | custom-call | flops 4294967296 | bytes 8000000 | tf_op jit(solution)/shard_map/pallas_call | solution.py:453
  288.3 4.3 %collective-permute-done.33.theirs_b = bf16[1024,1024]{1,0:T(8,128)(2,1)S(1)} collective-permute-done((bf16[1024,1024]{1,0:T(8,128)(2,1)}, bf16[1024,1024]{1,0:T(8,128)(2,1)S(1)}, u32[]{:S(2)}, u32[]{:S(2)}) %collective-permute-start.33) | collective-permute-done | bytes 2097184 | tf_op jit(solution)/shard_map/ppermute | solution.py:29
  294.2 5.2 %shard_map.140 = bf16[1024,1024]{1,0:T(8,128)(2,1)} custom-call(s32[4]{0:T(128)S(1)} %copy-done.6, bf16[1024,2048]{1,0:T(8,128)(2,1)S(1)} %copy-done, bf16[1024,1024]{1,0:T(8,128)(2,1)S(1)} %copy-done.3, bf16[1024,1024]{1,0:T(8,128)(2,1)} %collective-permute-done.30.theirs_a, bf16[1024,1024]{1,0:T(8,128)(2,1)S(1)} %copy-done.4, ...), custom_call_target="tpu_custom_call" | custom-call | flops 2000000000 | bytes 8000000 | tf_op jit(solution)/shard_map/pallas_call | solution.py:500
  (117 shorter events, 52.1 us)
Async XLA Ops:
  6.5 197.9 %all-gather.3.cloned.1.call-start = ((), (), s32[]{:S(2)}) async-start(), calls=%async_computation | async-start | bytes 4456448 | tf_op jit(solution)/shard_map/all_gather | solution.py:403
  16.8 36.8 %collective-permute-start = (bf16[1024,1024]{1,0:T(8,128)(2,1)}, bf16[1024,1024]{1,0:T(8,128)(2,1)}, u32[]{:S(2)}, u32[]{:S(2)}) collective-permute-start(bf16[1024,1024]{1,0:T(8,128)(2,1)} %bitcast.33), channel_id=1, source_target_pairs={{0,1},{1,0},{2,3},{3,2},{4,5},{5,4},{6,7},{7,6},{8,9},{9,8},{10,11... | collective-permute-start | bytes 6291464 | tf_op jit(solution)/shard_map/ppermute | solution.py:29
  18.9 15.3 %collective-permute-start.11 = (bf16[4,64,768]{2,1,0:T(8,128)(2,1)S(1)}, bf16[4,64,768]{2,1,0:T(8,128)(2,1)S(1)}, u32[]{:S(2)}, u32[]{:S(2)}) collective-permute-start(bf16[4,64,768]{2,1,0:T(8,128)(2,1)S(1)} %pad_maximum_fusion.3), channel_id=1, source_target_pairs={{0,2},{2,4},{4,6},{6,0},{1,3},{3,5},{5,7},{7,1},{8,10},{10,12},{12... | collective-permute-start | bytes 1179656 | tf_op jit(solution)/shard_map/ppermute | solution.py:29
  19.8 17.1 %collective-permute-start.12 = (bf16[4,64,768]{2,1,0:T(8,128)(2,1)S(1)}, bf16[4,64,768]{2,1,0:T(8,128)(2,1)S(1)}, u32[]{:S(2)}, u32[]{:S(2)}) collective-permute-start(bf16[4,64,768]{2,1,0:T(8,128)(2,1)S(1)} %pad_maximum_fusion.3), channel_id=1, source_target_pairs={{0,6},{2,0},{4,2},{6,4},{1,7},{3,1},{5,3},{7,5},{8,14},{10,8},{12,... | collective-permute-start | bytes 1179656 | tf_op jit(solution)/shard_map/ppermute | solution.py:29
  20.5 23.3 %collective-permute-start.13 = (bf16[4,64,768]{2,1,0:T(8,128)(2,1)S(1)}, bf16[4,64,768]{2,1,0:T(8,128)(2,1)S(1)}, u32[]{:S(2)}, u32[]{:S(2)}) collective-permute-start(bf16[4,64,768]{2,1,0:T(8,128)(2,1)S(1)} %pad_maximum_fusion.3), channel_id=1, source_target_pairs={{0,4},{2,6},{4,0},{6,2},{1,5},{3,7},{5,1},{7,3},{8,12},{10,14},{12... | collective-permute-start | bytes 1179656 | tf_op jit(solution)/shard_map/ppermute | solution.py:29
  22.1 26.2 %collective-permute-start.4 = (bf16[4,64,768]{2,1,0:T(8,128)(2,1)S(1)}, bf16[4,64,768]{2,1,0:T(8,128)(2,1)S(1)}, u32[]{:S(2)}, u32[]{:S(2)}) collective-permute-start(bf16[4,64,768]{2,1,0:T(8,128)(2,1)S(1)} %pad_maximum_fusion.2), channel_id=1, source_target_pairs={{0,8},{8,16},{16,24},{24,0},{1,9},{9,17},{17,25},{25,1},{2,10},{10... | collective-permute-start | bytes 1179656 | tf_op jit(solution)/shard_map/ppermute | solution.py:29
  34.3 14.8 %collective-permute-start.5 = (bf16[4,64,768]{2,1,0:T(8,128)(2,1)S(1)}, bf16[4,64,768]{2,1,0:T(8,128)(2,1)S(1)}, u32[]{:S(2)}, u32[]{:S(2)}) collective-permute-start(bf16[4,64,768]{2,1,0:T(8,128)(2,1)S(1)} %pad_maximum_fusion.2), channel_id=1, source_target_pairs={{0,24},{8,0},{16,8},{24,16},{1,25},{9,1},{17,9},{25,17},{2,26},{10... | collective-permute-start | bytes 1179656 | tf_op jit(solution)/shard_map/ppermute | solution.py:29
  36.9 13.0 %collective-permute-start.6 = (bf16[4,64,768]{2,1,0:T(8,128)(2,1)S(1)}, bf16[4,64,768]{2,1,0:T(8,128)(2,1)S(1)}, u32[]{:S(2)}, u32[]{:S(2)}) collective-permute-start(bf16[4,64,768]{2,1,0:T(8,128)(2,1)S(1)} %pad_maximum_fusion.2), channel_id=1, source_target_pairs={{0,16},{8,24},{16,0},{24,8},{1,17},{9,25},{17,1},{25,9},{2,18},{10... | collective-permute-start | bytes 1179656 | tf_op jit(solution)/shard_map/ppermute | solution.py:29
  44.6 37.0 %collective-permute-start.14 = (bf16[16,64,768]{2,1,0:T(8,128)(2,1)}, bf16[16,64,768]{2,1,0:T(8,128)(2,1)}, u32[]{:S(2)}, u32[]{:S(2)}) collective-permute-start(bf16[16,64,768]{2,1,0:T(8,128)(2,1)} %constant_dynamic-update-slice_fusion.7.refs_9_.refs_13_), channel_id=1, source_target_pairs={{0,96},{32,0},{64,32},{96,64},{1,97},{33,1},{65,33},{97,65},{2,98}... | collective-permute-start | bytes 4718600 | tf_op jit(solution)/shard_map/ppermute | solution.py:29
  50.7 30.9 %collective-permute-start.7 = (bf16[16,64,768]{2,1,0:T(8,128)(2,1)}, bf16[16,64,768]{2,1,0:T(8,128)(2,1)}, u32[]{:S(2)}, u32[]{:S(2)}) collective-permute-start(bf16[16,64,768]{2,1,0:T(8,128)(2,1)} %constant_dynamic-update-slice_fusion.refs_7_.refs_11_), channel_id=1, source_target_pairs={{0,32},{32,64},{64,96},{96,0},{1,33},{33,65},{65,97},{97,1},{2,34}... | collective-permute-start | bytes 4718600 | tf_op jit(solution)/shard_map/ppermute | solution.py:29
  105.9 123.9 %collective-permute-start.15 = (bf16[2,1024,1024]{2,1,0:T(8,128)(2,1)}, bf16[2,1024,1024]{2,1,0:T(8,128)(2,1)}, u32[]{:S(2)}, u32[]{:S(2)}) collective-permute-start(bf16[2,1024,1024]{2,1,0:T(8,128)(2,1)} %shard_map.137.refs_3_), channel_id=1, source_target_pairs={{0,1},{1,0},{2,3},{3,2},{4,5},{5,4},{6,7},{7,6},{8,9},{9,8},{10,11... | collective-permute-start | bytes 12582920 | tf_op jit(solution)/shard_map/ppermute | solution.py:29
  120.1 22.6 %collective-permute-start.18 = (bf16[2,64,1024]{2,1,0:T(8,128)(2,1)S(1)}, bf16[2,64,1024]{2,1,0:T(8,128)(2,1)S(1)}, u32[]{:S(2)}, u32[]{:S(2)}) collective-permute-start(bf16[2,64,1024]{2,1,0:T(8,128)(2,1)S(1)} %get-tuple-element.14), channel_id=1, source_target_pairs={{0,8},{8,16},{16,24},{24,0},{1,9},{9,17},{17,25},{25,1},{2,10},{10... | collective-permute-start | bytes 786440 | tf_op jit(solution)/shard_map/ppermute | solution.py:29
  135.6 31.5 %collective-permute-start.24 = (bf16[2,64,1024]{2,1,0:T(8,128)(2,1)S(1)}, bf16[2,64,1024]{2,1,0:T(8,128)(2,1)S(1)}, u32[]{:S(2)}, u32[]{:S(2)}) collective-permute-start(bf16[2,64,1024]{2,1,0:T(8,128)(2,1)S(1)} %get-tuple-element.13), channel_id=1, source_target_pairs={{0,2},{2,4},{4,6},{6,0},{1,3},{3,5},{5,7},{7,1},{8,10},{10,12},{12... | collective-permute-start | bytes 786440 | tf_op jit(solution)/shard_map/ppermute | solution.py:29
  144.2 57.3 %collective-permute-start.21 = (bf16[8,64,1024]{2,1,0:T(8,128)(2,1)S(1)}, bf16[8,64,1024]{2,1,0:T(8,128)(2,1)S(1)}, u32[]{:S(2)}, u32[]{:S(2)}) collective-permute-start(bf16[8,64,1024]{2,1,0:T(8,128)(2,1)S(1)} %pad_maximum_fusion.refs_6_), channel_id=1, source_target_pairs={{0,2},{2,4},{4,6},{6,0},{1,3},{3,5},{5,7},{7,1},{8,10},{10,12},{12... | collective-permute-start | bytes 3145736 | tf_op jit(solution)/shard_map/ppermute | solution.py:29
  151.5 50.1 %collective-permute-start.22 = (bf16[8,64,1024]{2,1,0:T(8,128)(2,1)S(1)}, bf16[8,64,1024]{2,1,0:T(8,128)(2,1)S(1)}, u32[]{:S(2)}, u32[]{:S(2)}) collective-permute-start(bf16[8,64,1024]{2,1,0:T(8,128)(2,1)S(1)} %pad_maximum_fusion.refs_6_), channel_id=1, source_target_pairs={{0,6},{2,0},{4,2},{6,4},{1,7},{3,1},{5,3},{7,5},{8,14},{10,8},{12,... | collective-permute-start | bytes 3145736 | tf_op jit(solution)/shard_map/ppermute | solution.py:29
  164.5 26.4 %collective-permute-start.25 = (bf16[2,64,1024]{2,1,0:T(8,128)(2,1)S(1)}, bf16[2,64,1024]{2,1,0:T(8,128)(2,1)S(1)}, u32[]{:S(2)}, u32[]{:S(2)}) collective-permute-start(bf16[2,64,1024]{2,1,0:T(8,128)(2,1)S(1)} %get-tuple-element.13), channel_id=1, source_target_pairs={{0,6},{2,0},{4,2},{6,4},{1,7},{3,1},{5,3},{7,5},{8,14},{10,8},{12,... | collective-permute-start | bytes 786440 | tf_op jit(solution)/shard_map/ppermute | solution.py:29
  167.1 31.9 %collective-permute-start.26 = (bf16[2,64,1024]{2,1,0:T(8,128)(2,1)S(1)}, bf16[2,64,1024]{2,1,0:T(8,128)(2,1)S(1)}, u32[]{:S(2)}, u32[]{:S(2)}) collective-permute-start(bf16[2,64,1024]{2,1,0:T(8,128)(2,1)S(1)} %get-tuple-element.13), channel_id=1, source_target_pairs={{0,4},{2,6},{4,0},{6,2},{1,5},{3,7},{5,1},{7,3},{8,12},{10,14},{12... | collective-permute-start | bytes 786440 | tf_op jit(solution)/shard_map/ppermute | solution.py:29
  190.9 21.3 %collective-permute-start.23 = (bf16[8,64,1024]{2,1,0:T(8,128)(2,1)S(1)}, bf16[8,64,1024]{2,1,0:T(8,128)(2,1)}, u32[]{:S(2)}, u32[]{:S(2)}) collective-permute-start(bf16[8,64,1024]{2,1,0:T(8,128)(2,1)S(1)} %pad_maximum_fusion.refs_6_), channel_id=1, source_target_pairs={{0,4},{2,6},{4,0},{6,2},{1,5},{3,7},{5,1},{7,3},{8,12},{10,14},{12... | collective-permute-start | bytes 3145736 | tf_op jit(solution)/shard_map/ppermute | solution.py:29
  200.0 23.2 %collective-permute-start.27 = (bf16[8,64,1024]{2,1,0:T(8,128)(2,1)}, bf16[8,64,1024]{2,1,0:T(8,128)(2,1)}, u32[]{:S(2)}, u32[]{:S(2)}) collective-permute-start(bf16[8,64,1024]{2,1,0:T(8,128)(2,1)} %pad_maximum_fusion.1.refs_10_), channel_id=1, source_target_pairs={{0,8},{8,16},{16,24},{24,0},{1,9},{9,17},{17,25},{25,1},{2,10},{10... | collective-permute-start | bytes 3145736 | tf_op jit(solution)/shard_map/ppermute | solution.py:29
  201.6 27.1 %collective-permute-start.28 = (bf16[8,64,1024]{2,1,0:T(8,128)(2,1)}, bf16[8,64,1024]{2,1,0:T(8,128)(2,1)}, u32[]{:S(2)}, u32[]{:S(2)}) collective-permute-start(bf16[8,64,1024]{2,1,0:T(8,128)(2,1)} %pad_maximum_fusion.1.refs_10_), channel_id=1, source_target_pairs={{0,24},{8,0},{16,8},{24,16},{1,25},{9,1},{17,9},{25,17},{2,26},{10... | collective-permute-start | bytes 3145736 | tf_op jit(solution)/shard_map/ppermute | solution.py:29
  203.5 26.3 %collective-permute-start.29 = (bf16[8,64,1024]{2,1,0:T(8,128)(2,1)}, bf16[8,64,1024]{2,1,0:T(8,128)(2,1)}, u32[]{:S(2)}, u32[]{:S(2)}) collective-permute-start(bf16[8,64,1024]{2,1,0:T(8,128)(2,1)} %pad_maximum_fusion.1.refs_10_), channel_id=1, source_target_pairs={{0,16},{8,24},{16,0},{24,8},{1,17},{9,25},{17,1},{25,9},{2,18},{10... | collective-permute-start | bytes 3145736 | tf_op jit(solution)/shard_map/ppermute | solution.py:29
  212.2 65.7 %collective-permute-start.31 = (bf16[8,64,2048]{2,1,0:T(8,128)(2,1)}, bf16[8,64,2048]{2,1,0:T(8,128)(2,1)}, u32[]{:S(2)}, u32[]{:S(2)}) collective-permute-start(bf16[8,64,2048]{2,1,0:T(8,128)(2,1)} %bitcast.14), channel_id=1, source_target_pairs={{0,32},{32,64},{64,96},{96,0},{1,33},{33,65},{65,97},{97,1},{2,34}... | collective-permute-start | bytes 6291464 | tf_op jit(solution)/shard_map/ppermute | solution.py:29
  223.3 54.6 %collective-permute-start.32 = (bf16[8,64,2048]{2,1,0:T(8,128)(2,1)S(1)}, bf16[8,64,2048]{2,1,0:T(8,128)(2,1)}, u32[]{:S(2)}, u32[]{:S(2)}) collective-permute-start(bf16[8,64,2048]{2,1,0:T(8,128)(2,1)S(1)} %bitcast.39), channel_id=1, source_target_pairs={{0,96},{32,0},{64,32},{96,64},{1,97},{33,1},{65,33},{97,65},{2,98}... | collective-permute-start | bytes 6291464 | tf_op jit(solution)/shard_map/ppermute | solution.py:29
  255.4 32.8 %collective-permute-start.30 = (bf16[1024,1024]{1,0:T(8,128)(2,1)}, bf16[1024,1024]{1,0:T(8,128)(2,1)}, u32[]{:S(2)}, u32[]{:S(2)}) collective-permute-start(bf16[1024,1024]{1,0:T(8,128)(2,1)} %get-tuple-element.9.mine_a), channel_id=1, source_target_pairs={{0,1},{1,0},{2,3},{3,2},{4,5},{5,4},{6,7},{7,6},{8,9},{9,8},{10,11... | collective-permute-start | bytes 6291464 | tf_op jit(solution)/shard_map/ppermute | solution.py:29
  (26 other events, 309.9 us)
Sparse Core Ops, SparseCore 0:
  9.5 61.5 all-gather.2

commit v2 on v1

--- a/solution.py
+++ b/solution.py
@@ -57,15 +57,6 @@
 def whole_ring(v, places, axis):
     pieces = ring_pieces(v, places, axis)
     return jnp.concatenate([p for p, _ in pieces], axis=0), sum((q for _, q in pieces), [])
-
-
-def plane_pieces(own, first, width):
-    half = own.shape[0] // 2
-    places = [(i % 4, i // 4, 0, 1, 0) for i in range(2 * half)]
-    lower = step(own[:half, :, first : first + width], "z", 1)
-    upper = step(own[half:, :, first : first + width], "z", 3)
-    far = moved(places, "z", 1)
-    return [(own, places, first), (lower, far[:half]), (upper, far[half:])]
 
 
 def start_weights(refs, layout, pos, target, sem, plane=None):
@@ -85,6 +76,19 @@
             ).start()
 
 
+def sort_kernel(*refs):
+    pieces, (down, up), sem = refs[:4], refs[4:6], refs[6]
+    copies = []
+    for k, piece in enumerate(pieces):
+        copies.append((piece.at[4:6], up.at[2 * k : 2 * k + 2], sem.at[2 * k]))
+        copies.append((piece.at[0:4], down.at[4 * k : 4 * k + 4], sem.at[2 * k + 1]))
+    copies = [pltpu.make_async_copy(*c) for c in copies]
+    for c in copies:
+        c.start()
+    for c in copies:
+        c.wait()
+
+
 def norm_kernel(own, other, gain, normed):
     def rows(i, _):
         s = pl.ds(pl.multiple_of(i * TILE, TILE), TILE)
@@ -110,38 +114,37 @@
     padded[:8, :] = jnp.zeros((8, channels), f32)
     blocks, block = recur_gate.shape[0], recur_gate.shape[1]
     pltpu.make_async_copy(entry, entry, in_sem).wait()
-    for r in range(0, length, TILE):
-        both = jnp.dot(normed[r : r + TILE, :], entry[...], preferred_element_type=f32)
-        both = both.astype(bf16)
-        gate[r : r + TILE, :] = both[:, :channels]
-        padded[8 + r : 8 + r + TILE, :] = both[:, channels:].astype(f32)
-        acc = padded[r + 5 : r + 5 + TILE, :] * taps[0:1, :]
+
+    def enter(i, _):
+        s = pl.ds(pl.multiple_of(i * TILE, TILE), TILE)
+        both = jnp.dot(normed[s, :], entry[...], preferred_element_type=f32).astype(bf16)
+        gate[s, :] = both[:, :channels]
+        padded[pl.ds(pl.multiple_of(8 + i * TILE, 8), TILE), :] = both[:, channels:].astype(f32)
+        window = padded[pl.ds(pl.multiple_of(i * TILE, TILE), TILE + 8), :]
+        acc = window[5 : 5 + TILE, :] * taps[0:1, :]
         for k in range(1, 4):
-            acc = acc + padded[r + 5 + k : r + 5 + k + TILE, :] * taps[k : k + 1, :]
+            acc = acc + window[5 + k : 5 + k + TILE, :] * taps[k : k + 1, :]
         filt = acc.astype(bf16)
         for n_b in range(blocks):
             cols = slice(n_b * block, (n_b + 1) * block)
             fb = filt[:, cols]
             recur = jax.nn.sigmoid(jnp.dot(fb, recur_gate[n_b], preferred_element_type=f32))
             inlet = jax.nn.sigmoid(jnp.dot(fb, inlet_gate[n_b], preferred_element_type=f32))
-            log_decay = shift[r : r + TILE, :] - recur * rate[:, cols]
+            log_decay = shift[s, :] - recur * rate[:, cols]
             a = jnp.exp(log_decay)
             t = 2.0 * log_decay
-            series = -t * (
-                1.0
-                + t
-                * (
-                    1.0 / 2
-                    + t
-                    * (1.0 / 6 + t * (1.0 / 24 + t * (1.0 / 120 + t * (1.0 / 720 + t / 5040))))
-                )
-            )
+            series = 1.0 / 120 + t * (1.0 / 720 + t / 5040)
+            series = 1.0 / 2 + t * (1.0 / 6 + t * (1.0 / 24 + t * series))
+            series = -t * (1.0 + t * series)
             gone = jnp.where(t > -0.4, series, 1.0 - a * a)
             into = jnp.sqrt(gone) * inlet * fb.astype(f32)
             for q in range(block // 128):
                 at = n_b * (block // 128) + q
-                decay[at, r : r + TILE, :] = a[:, q * 128 : q * 128 + 128]
-                drive[at, r : r + TILE, :] = into[:, q * 128 : q * 128 + 128]
+                decay[at, s, :] = a[:, q * 128 : q * 128 + 128]
+                drive[at, s, :] = into[:, q * 128 : q * 128 + 128]
+        return 0
+
+    lax.fori_loop(0, length // TILE, enter, 0)
     seg = length // SEGS
 
     def scan(j, carry):
@@ -161,12 +164,12 @@
     lanes = channels // 128
     zero, one = jnp.zeros((SEGS, 128), f32), jnp.ones((SEGS, 128), f32)
     lax.fori_loop(0, seg, scan, ((zero,) * lanes, (one,) * lanes), unroll=8)
-    carry = [jnp.zeros((1, 128), f32)] * lanes
     pltpu.make_async_copy(weights, weights, weight_sem).wait()
-    for r in range(0, length, TILE):
-        rows = []
-        for i in range(r, r + TILE, seg):
-            s = slice(i, i + seg)
+
+    def leave(r, carry):
+        carry, rows = list(carry), []
+        for i in range(TILE // seg):
+            s = pl.ds(pl.multiple_of(r * TILE + i * seg, seg), seg)
             row = []
             for q in range(lanes):
                 states = drive[q, s, :] + prod[q, s, :] * carry[q]
@@ -177,19 +180,22 @@
                 row.append((states * branch).astype(bf16))
             rows.append(jnp.concatenate(row, axis=1))
         left = jnp.concatenate(rows, axis=0)
-        s = slice(r, r + TILE)
+        s = pl.ds(pl.multiple_of(r * TILE, TILE), TILE)
         for h in range(2):
             half = weights[h * HALF : h * HALF + HALF, :]
             part[h, s, :] = dot_turned(left, half).astype(bf16)
             pltpu.make_async_copy(part.at[h, s, :], part_out.at[h, s, :], out_sem).start()
+        return tuple(carry)
+
+    lax.fori_loop(0, length // TILE, leave, (jnp.zeros((1, 128), f32),) * lanes)
     pltpu.make_async_copy(part, part_out, out_sem).wait()
 
 
 def turned_kernel(layout, plane, *refs):
     n = len(layout)
     pos, left_in = refs[:2]
-    pieces, out_ref = refs[2 : 2 + n], refs[2 + n]
-    left, weights, out, sem, in_sem, out_sem = refs[3 + n :]
+    pieces, out = refs[2 : 2 + n], refs[2 + n]
+    left, weights, sem, in_sem = refs[3 + n :]
     tiles = out.shape[0] // TILE
 
     def arriving(t):
@@ -206,11 +212,9 @@
         arriving(t).wait()
         s = pl.ds(pl.multiple_of(t * TILE, TILE), TILE)
         out[s, :] = dot_turned(left[s, :], weights[...]).astype(bf16)
-        pltpu.make_async_copy(out.at[s, :], out_ref.at[s, :], out_sem).start()
         return 0
 
     lax.fori_loop(0, tiles, rows, 0)
-    pltpu.make_async_copy(out, out_ref, out_sem).wait()
 
 
 def dot_turned(left, right):
@@ -222,13 +226,12 @@
     n, m = len(layout), len(down_layout)
     pieces, down_pieces = refs[6 : 6 + n], refs[6 + n : 6 + n + m]
     mid_out, act_out, part_out = refs[6 + n + m : 9 + n + m]
-    stream, parts, up, down, mid, act, part = refs[9 + n + m : 16 + n + m]
+    stream, parts, up, down, normed, mid, act, part = refs[9 + n + m : 17 + n + m]
+    up_sem, down_sem, in_sem, act_sem, mid_sem, part_sem = refs[17 + n + m :]
     tiles = own.shape[0] // TILE
-    normed = refs[16 + n + m : 16 + n + m + tiles]
-    up_sem, down_sem, in_sem, act_sem, mid_sem, part_sem = refs[16 + n + m + tiles :]
 
     def arriving(t):
-        s = slice(t * TILE, (t + 1) * TILE)
+        s = pl.ds(pl.multiple_of(t * TILE, TILE), TILE)
         pairs = [
             (own, stream.at[0]),
             (other, stream.at[1]),
@@ -242,10 +245,20 @@
             for k, (src, dst) in enumerate(pairs)
         ]
 
-    def norm(t):
+    for c in arriving(0):
+        c.start()
+    start_weights(pieces, layout, pos, up, up_sem)
+    for c in arriving(1):
+        c.start()
+    start_weights(down_pieces, down_layout, pos, down, down_sem, 0)
+    for t in range(2, tiles):
+        for c in arriving(t):
+            c.start()
+
+    def rows(t, _):
         for c in arriving(t):
             c.wait()
-        s = slice(t * TILE, (t + 1) * TILE)
+        s = pl.ds(pl.multiple_of(t * TILE, TILE), TILE)
         halves = []
         for h in range(2):
             v = stream[h, s, :].astype(f32) + (
@@ -257,33 +270,24 @@
         a, b = halves
         ms = (jnp.sum(a * a, -1, keepdims=True) + jnp.sum(b * b, -1, keepdims=True)) / D
         r = lax.rsqrt(ms + epsilon)
-        normed[t][:, :HALF] = (a * r * gain[:, :HALF]).astype(bf16)
-        normed[t][:, HALF:] = (b * r * gain[:, HALF:]).astype(bf16)
+        normed[:, :HALF] = (a * r * gain[:, :HALF]).astype(bf16)
+        normed[:, HALF:] = (b * r * gain[:, HALF:]).astype(bf16)
         pltpu.make_async_copy(mid.at[s, :], mid_out.at[s, :], mid_sem).start()
 
-    for c in arriving(0):
-        c.start()
-    start_weights(pieces, layout, pos, up, up_sem)
-    for c in arriving(1):
-        c.start()
-    start_weights(down_pieces, down_layout, pos, down, down_sem, 0)
-    for t in range(2, tiles):
-        for c in arriving(t):
-            c.start()
-    norm(0)
-    pltpu.make_async_copy(up, up, up_sem).wait()
-    for t in range(tiles):
-        s = slice(t * TILE, (t + 1) * TILE)
-        if t + 1 < tiles:
-            norm(t + 1)
-        prod = jnp.dot(normed[t][...], up[...], preferred_element_type=f32)
+        @pl.when(t == 0)
+        def _():
+            pltpu.make_async_copy(up, up, up_sem).wait()
+            pltpu.make_async_copy(down, down, down_sem).wait()
+
+        prod = jnp.dot(normed[...], up[...], preferred_element_type=f32)
         left = jnp.square(jnp.maximum(prod, 0.0)).astype(bf16)
         act[s, :] = left
         pltpu.make_async_copy(act.at[s, :], act_out.at[s, :], act_sem).start()
-        if t == 0:
-            pltpu.make_async_copy(down, down, down_sem).wait()
         part[s, :] = dot_turned(left, down[...]).astype(bf16)
         pltpu.make_async_copy(part.at[s, :], part_out.at[s, :], part_sem).start()
+        return 0
+
+    lax.fori_loop(0, tiles, rows, 0)
     pltpu.make_async_copy(mid, mid_out, mid_sem).wait()
     pltpu.make_async_copy(act, act_out, act_sem).wait()
     pltpu.make_async_copy(part, part_out, part_sem).wait()
@@ -386,22 +390,41 @@
 
     mid_col, part = hidden // 2, channels // 2
     mixer_t, down_t = mixer_out.T, down_weight.T
-    here = [(0, 0, 0, 0, 0)]
-    left = jnp.concatenate([gate_weight, mixer_t[:, :part]], axis=1)[None]
-    right = jnp.concatenate([mixer_t[:, part:], input_weight], axis=1)[None]
-    by_x = whole_ring(left, here, "x")
-    by_y = whole_ring(right, here, "y")
+    here, wide = [(0, 0, 0, 0, 0)], channels + part
+    left = [gate_weight, mixer_t[:, :part], down_t[:, :mid_col]]
+    right = [mixer_t[:, part:], input_weight, down_t[:, mid_col:]]
+    by_x, at_x = whole_ring(jnp.concatenate(left, axis=1)[None], here, "x")
+    by_y, at_y = whole_ring(jnp.concatenate(right, axis=1)[None], here, "y")
     pair, places = both_planes(up_weight)
-    by_xy = whole_ring(*by_x, "y")
-    by_yx = whole_ring(*by_y, "x")
+    by_xy = whole_ring(by_x[:, :, :wide], at_x, "y")
+    by_yx = whole_ring(by_y[:, :, :wide], at_y, "x")
     x_pieces = [by_xy, (step(by_xy[0], "z", 1), moved(by_xy[1], "z", 1))]
     y_pieces = [by_yx, (step(by_yx[0], "z", 3), moved(by_yx[1], "z", 1))]
-    later = whole_ring(pair[:, :, :mid_col], places, "y")
-    up_x = ring_pieces(*later, "x")
-    later = whole_ring(pair[:, :, mid_col:], places, "x")
-    up_y = ring_pieces(*later, "y")
-    plane = lax.all_gather(down_t, ("y", "x"), axis=0, tiled=False)
-    down_pieces = plane_pieces(plane, 0, hidden)
+
+    def later(ring, at, cols, axis):
+        both = jnp.concatenate([ring[:, :, wide:], pair[:, :, cols]], axis=0)
+        pieces = ring_pieces(both, at + places, axis)
+        block = both.shape[1:]
+        split = call(
+            sort_kernel,
+            (jax.ShapeDtypeStruct((16, *block), bf16), jax.ShapeDtypeStruct((8, *block), bf16)),
+            [HBM] * 4,
+            1e6,
+            [pltpu.SemaphoreType.DMA((8,))],
+            VMEM,
+            16,
+        )(*[v for v, _ in pieces])
+        return [
+            (v, sum((p[s] for _, p in pieces), []))
+            for v, s in zip(split, (slice(0, 4), slice(4, 6)))
+        ]
+
+    down_a, up_a = later(by_x, at_x, slice(0, mid_col), "y")
+    down_b, up_b = later(by_y, at_y, slice(mid_col, hidden), "x")
+    up_x = ring_pieces(*up_a, "x")
+    up_y = ring_pieces(*up_b, "y")
+    far_a = (step(down_a[0], "z", 1), moved(down_a[1], "z", 1))
+    far_b = (step(down_b[0], "z", 3), moved(down_b[1], "z", 1))
 
     shape = jax.ShapeDtypeStruct
     whole, one_half = shape((length, D), bf16), shape((length, HALF), bf16)
@@ -448,8 +471,12 @@
     theirs = step(mine, "tp", 1)
     tiles = length // TILE
 
-    def turned(left, pieces, plane):
-        arrays, layout = flat(pieces, 0, left.shape[1])
+    def halves(low, high):
+        (a, la), (b, lb) = flat(low, 0, mid_col), flat(high, mid_col, mid_col)
+        return a + b, la + lb
+
+    def turned(left, low, high, plane):
+        arrays, layout = halves(low, high)
         return call(
             functools.partial(turned_kernel, layout, plane),
             one_half,
@@ -458,17 +485,16 @@
             [
                 pltpu.VMEM(left.shape, bf16),
                 pltpu.VMEM((HALF, left.shape[1]), bf16),
-                pltpu.VMEM((length, HALF), bf16),
                 pltpu.SemaphoreType.DMA,
                 pltpu.SemaphoreType.DMA((tiles,)),
-                pltpu.SemaphoreType.DMA,
             ],
-            HBM,
+            VMEM,
+            24,
         )(pos, left, *arrays)
 
     a, la = flat(up_x, 0, mid_col)
     b, lb = flat(up_y, mid_col, mid_col)
-    c, lc = flat(down_pieces[:1], 0, hidden)
+    c, lc = halves([down_a], [down_b])
     mid, activated, mine_c = call(
         functools.partial(ffn_kernel, la + lb, lc),
         (whole, shape((length, hidden), bf16), one_half),
@@ -479,12 +505,10 @@
             pltpu.VMEM((2, 2, length, HALF), bf16),
             pltpu.VMEM((D, hidden), bf16),
             pltpu.VMEM((HALF, hidden), bf16),
+            pltpu.VMEM((TILE, D), bf16),
             pltpu.VMEM((length, D), bf16),
             pltpu.VMEM((length, hidden), bf16),
             pltpu.VMEM((length, HALF), bf16),
-        ]
-        + [pltpu.VMEM((TILE, D), bf16)] * tiles
-        + [
             pltpu.SemaphoreType.DMA,
             pltpu.SemaphoreType.DMA,
             pltpu.SemaphoreType.DMA((tiles, 6)),
@@ -495,7 +519,7 @@
         HBM,
     )(pos, own, other, mine, theirs, own_first(feedforward_gain), *a, *b, *c)
     theirs_c = step(mine_c, "tp", 1)
-    mine_d = turned(activated, down_pieces[1:], 1)
+    mine_d = turned(activated, [far_a], [far_b], 1)
     theirs_d = step(mine_d, "tp", 1)
     out = call(
         closing_kernel,

time: 311 us -> 299 us (0.961)
  the two profiles are of different devices: /device:TPU:19 before, /device:TPU:1 now
where the time goes in v2:
time: 299 us; the launch traced here: 298 us
  waiting for transfers between devices  120 us (40%)
  starting transfers between devices  91.9 us (31%)
  Pallas kernels  70.3 us (24%)
  local copies, waits for them, and re-layouts  9.57 us (3%)
  other arithmetic  5.86 us (2%)
    ppermute x34, waiting for transfers between devices, step(): return lax.ppermute(v, over, [(i, (i + shift) % size) for i in range(size)])  120 us
    ppermute x34, starting transfers between devices, step(): return lax.ppermute(v, over, [(i, (i + shift) % size) for i in range(size)])  91.9 us
    pallas_call x1, Pallas kernels, local(): call(functools.partial(ffn_kernel, la + lb, lc), (whole, shape((length, h...  26.3 us
    pallas_call x1, Pallas kernels, local(): call(functools.partial(mixer_kernel, la + lb, lc + ld), partial, [SMEM] +...  25.4 us
    pallas_call x1, Pallas kernels, turned(): call(functools.partial(turned_kernel, layout, plane), one_half, [SMEM, HB...  8.29 us
    unnamed x46, local copies, waits for them, and re-layouts  6.14 us
  transfers between devices with their start and end apart: 34, of which 16 were waited for; matrix products, arithmetic and copies ran while one was open for 2% of the time, Pallas kernels for 11%

profile of v2, /device:TPU:1, one launch (start us, length us, event | category | flops | bytes accessed | tf_op | source)
XLA Modules:
  0.0 298.3 jit_solution(9514568532434692993)
XLA Ops:
  2.8 3.8 %collective-permute-start.10 = (bf16[1,64,1792]{2,1,0:T(8,128)(2,1)S(1)}, bf16[1,64,1792]{2,1,0:T(8,128)(2,1)S(1)}, u32[]{:S(2)}, u32[]{:S(2)}) collective-permute-start(bf16[1,64,1792]{2,1,0:T(8,128)(2,1)S(1)} %maximum_bitcast_fusion.2), channel_id=1, source_target_pairs={{0,16},{8,24},{16,0},{24,8},{1,17},{9,25},{17,1},{25,9},{2,18},{10... | collective-permute-start | bytes 688136 | tf_op jit(solution)/shard_map/ppermute | solution.py:29
  11.7 5.9 %collective-permute-done.8 = bf16[1,64,1792]{2,1,0:T(8,128)(2,1)S(1)} collective-permute-done((bf16[1,64,1792]{2,1,0:T(8,128)(2,1)S(1)}, bf16[1,64,1792]{2,1,0:T(8,128)(2,1)S(1)}, u32[]{:S(2)}, u32[]{:S(2)}) %collective-permute-start.8) | collective-permute-done | bytes 229408 | tf_op jit(solution)/shard_map/ppermute | solution.py:29
  24.2 9.2 %collective-permute-done.2 = bf16[1,64,1792]{2,1,0:T(8,128)(2,1)S(1)} collective-permute-done((bf16[1,64,1792]{2,1,0:T(8,128)(2,1)S(1)}, bf16[1,64,1792]{2,1,0:T(8,128)(2,1)S(1)}, u32[]{:S(2)}, u32[]{:S(2)}) %collective-permute-start.2) | collective-permute-done | bytes 229408 | tf_op jit(solution)/shard_map/ppermute | solution.py:29
  43.3 3.3 %collective-permute-start.14 = (bf16[16,64,768]{2,1,0:T(8,128)(2,1)}, bf16[16,64,768]{2,1,0:T(8,128)(2,1)}, u32[]{:S(2)}, u32[]{:S(2)}) collective-permute-start(bf16[16,64,768]{2,1,0:T(8,128)(2,1)} %pad_maximum_fusion.1.refs_9_.refs_13_), channel_id=1, source_target_pairs={{0,96},{32,0},{64,32},{96,64},{1,97},{33,1},{65,33},{97,65},{2,98}... | collective-permute-start | bytes 4718600 | tf_op jit(solution)/shard_map/ppermute | solution.py:29
  60.5 8.6 %collective-permute-done.14.refs_10_.refs_14_ = bf16[16,64,768]{2,1,0:T(8,128)(2,1)} collective-permute-done((bf16[16,64,768]{2,1,0:T(8,128)(2,1)}, bf16[16,64,768]{2,1,0:T(8,128)(2,1)}, u32[]{:S(2)}, u32[]{:S(2)}) %collective-permute-start.14) | collective-permute-done | bytes 1572896 | tf_op jit(solution)/shard_map/ppermute | solution.py:29
  69.1 12.3 %collective-permute-done.7.refs_8_.refs_12_ = bf16[16,64,768]{2,1,0:T(8,128)(2,1)} collective-permute-done((bf16[16,64,768]{2,1,0:T(8,128)(2,1)}, bf16[16,64,768]{2,1,0:T(8,128)(2,1)}, u32[]{:S(2)}, u32[]{:S(2)}) %collective-permute-start.7) | collective-permute-done | bytes 1572896 | tf_op jit(solution)/shard_map/ppermute | solution.py:29
  81.4 25.4 %shard_map.137.refs_3_ = bf16[2,1024,1024]{2,1,0:T(8,128)(2,1)} custom-call(s32[4]{0:T(128)} %pad_add_fusion.refs_0_.pos, bf16[1024,2048]{1,0:T(8,128)(2,1)} %copy-done.1, f32[4,512]{1,0:T(4,128)} %refs_2_.1, bf16[2,256,256]{2,1,0:T(8,128)(2,1)} %refs_3_.1, bf16[2,256,256]{2,1,0:T(8,128)(2,1)} %refs_4_.1, f32[1,512]{1,0:T(1,128)} %bitcast.37, ...), custom_call_target="tpu_custom_call" | custom-call | flops 12000000000 | bytes 8000000 | tf_op jit(solution)/shard_map/pallas_call | solution.py:439
  106.8 9.3 %collective-permute-start.15 = (bf16[2,1024,1024]{2,1,0:T(8,128)(2,1)}, bf16[2,1024,1024]{2,1,0:T(8,128)(2,1)}, u32[]{:S(2)}, u32[]{:S(2)}) collective-permute-start(bf16[2,1024,1024]{2,1,0:T(8,128)(2,1)} %shard_map.137.refs_3_), channel_id=1, source_target_pairs={{0,1},{1,0},{2,3},{3,2},{4,5},{5,4},{6,7},{7,6},{8,9},{9,8},{10,11... | collective-permute-start | bytes 12582920 | tf_op jit(solution)/shard_map/ppermute | solution.py:29
  118.8 3.6 %collective-permute-done.16 = bf16[32,2048]{1,0:T(8,128)(2,1)S(1)} collective-permute-done((bf16[32,2048]{1,0:T(8,128)(2,1)S(1)}, bf16[32,2048]{1,0:T(8,128)(2,1)S(1)}, u32[]{:S(2)}, u32[]{:S(2)}) %collective-permute-start.16) | collective-permute-done | bytes 131104 | tf_op jit(solution)/shard_map/ppermute | solution.py:29
  125.4 4.5 %collective-permute-start.24 = (bf16[6,64,1024]{2,1,0:T(8,128)(2,1)S(1)}, bf16[6,64,1024]{2,1,0:T(8,128)(2,1)S(1)}, u32[]{:S(2)}, u32[]{:S(2)}) collective-permute-start(bf16[6,64,1024]{2,1,0:T(8,128)(2,1)S(1)} %fusion.refs_0_), channel_id=1, source_target_pairs={{0,2},{2,4},{4,6},{6,0},{1,3},{3,5},{5,7},{7,1},{8,10},{10,12},{12... | collective-permute-start | bytes 2359304 | tf_op jit(solution)/shard_map/ppermute | solution.py:29
  129.9 12.3 %collective-permute-done.18.refs_1_ = bf16[6,64,1024]{2,1,0:T(8,128)(2,1)S(1)} collective-permute-done((bf16[6,64,1024]{2,1,0:T(8,128)(2,1)S(1)}, bf16[6,64,1024]{2,1,0:T(8,128)(2,1)S(1)}, u32[]{:S(2)}, u32[]{:S(2)}) %collective-permute-start.18) | collective-permute-done | bytes 786464 | tf_op jit(solution)/shard_map/ppermute | solution.py:29
  142.2 6.3 %collective-permute-start.25 = (bf16[6,64,1024]{2,1,0:T(8,128)(2,1)S(1)}, bf16[6,64,1024]{2,1,0:T(8,128)(2,1)S(1)}, u32[]{:S(2)}, u32[]{:S(2)}) collective-permute-start(bf16[6,64,1024]{2,1,0:T(8,128)(2,1)S(1)} %fusion.refs_0_), channel_id=1, source_target_pairs={{0,6},{2,0},{4,2},{6,4},{1,7},{3,1},{5,3},{7,5},{8,14},{10,8},{12,... | collective-permute-start | bytes 2359304 | tf_op jit(solution)/shard_map/ppermute | solution.py:29
  148.5 10.4 %collective-permute-done.20.refs_3_ = bf16[6,64,1024]{2,1,0:T(8,128)(2,1)S(1)} collective-permute-done((bf16[6,64,1024]{2,1,0:T(8,128)(2,1)S(1)}, bf16[6,64,1024]{2,1,0:T(8,128)(2,1)S(1)}, u32[]{:S(2)}, u32[]{:S(2)}) %collective-permute-start.20) | collective-permute-done | bytes 786464 | tf_op jit(solution)/shard_map/ppermute | solution.py:29
  159.2 4.4 %collective-permute-start.21 = (bf16[8,64,1024]{2,1,0:T(8,128)(2,1)S(1)}, bf16[8,64,1024]{2,1,0:T(8,128)(2,1)S(1)}, u32[]{:S(2)}, u32[]{:S(2)}) collective-permute-start(bf16[8,64,1024]{2,1,0:T(8,128)(2,1)S(1)} %get-tuple-element.12.refs_6_), channel_id=1, source_target_pairs={{0,2},{2,4},{4,6},{6,0},{1,3},{3,5},{5,7},{7,1},{8,10},{10,12},{12... | collective-permute-start | bytes 3145736 | tf_op jit(solution)/shard_map/ppermute | solution.py:29
  165.8 4.5 %collective-permute-start.23 = (bf16[8,64,1024]{2,1,0:T(8,128)(2,1)S(1)}, bf16[8,64,1024]{2,1,0:T(8,128)(2,1)S(1)}, u32[]{:S(2)}, u32[]{:S(2)}) collective-permute-start(bf16[8,64,1024]{2,1,0:T(8,128)(2,1)S(1)} %get-tuple-element.12.refs_6_), channel_id=1, source_target_pairs={{0,4},{2,6},{4,0},{6,2},{1,5},{3,7},{5,1},{7,3},{8,12},{10,14},{12... | collective-permute-start | bytes 3145736 | tf_op jit(solution)/shard_map/ppermute | solution.py:29
  172.4 25.9 %collective-permute-done.21.refs_7_ = bf16[8,64,1024]{2,1,0:T(8,128)(2,1)S(1)} collective-permute-done((bf16[8,64,1024]{2,1,0:T(8,128)(2,1)S(1)}, bf16[8,64,1024]{2,1,0:T(8,128)(2,1)S(1)}, u32[]{:S(2)}, u32[]{:S(2)}) %collective-permute-start.21) | collective-permute-done | bytes 1048608 | tf_op jit(solution)/shard_map/ppermute | solution.py:29
  198.3 5.1 %collective-permute-start.28 = (bf16[8,64,1024]{2,1,0:T(8,128)(2,1)}, bf16[8,64,1024]{2,1,0:T(8,128)(2,1)}, u32[]{:S(2)}, u32[]{:S(2)}) collective-permute-start(bf16[8,64,1024]{2,1,0:T(8,128)(2,1)} %get-tuple-element.13.refs_10_), channel_id=1, source_target_pairs={{0,24},{8,0},{16,8},{24,16},{1,25},{9,1},{17,9},{25,17},{2,26},{10... | collective-permute-start | bytes 3145736 | tf_op jit(solution)/shard_map/ppermute | solution.py:29
  204.9 3.7 %collective-permute-done.23.refs_9_ = bf16[8,64,1024]{2,1,0:T(8,128)(2,1)S(1)} collective-permute-done((bf16[8,64,1024]{2,1,0:T(8,128)(2,1)S(1)}, bf16[8,64,1024]{2,1,0:T(8,128)(2,1)S(1)}, u32[]{:S(2)}, u32[]{:S(2)}) %collective-permute-start.23) | collective-permute-done | bytes 1048608 | tf_op jit(solution)/shard_map/ppermute | solution.py:29
  213.1 16.4 %collective-permute-done.28.refs_12_ = bf16[8,64,1024]{2,1,0:T(8,128)(2,1)} collective-permute-done((bf16[8,64,1024]{2,1,0:T(8,128)(2,1)}, bf16[8,64,1024]{2,1,0:T(8,128)(2,1)}, u32[]{:S(2)}, u32[]{:S(2)}) %collective-permute-start.28) | collective-permute-done | bytes 1048608 | tf_op jit(solution)/shard_map/ppermute | solution.py:29
  229.5 26.3 %shard_map.140 = (bf16[1024,2048]{1,0:T(8,128)(2,1)}, bf16[1024,2048]{1,0:T(8,128)(2,1)}, bf16[1024,1024]{1,0:T(8,128)(2,1)}) custom-call(s32[4]{0:T(128)} %pad_add_fusion.refs_0_.pos, bf16[1024,1024]{1,0:T(8,128)(2,1)} %bitcast.26, bf16[1024,1024]{1,0:T(8,128)(2,1)} %collective-permute-done.other.refs_2_, bf16[2,1024,1024]{2,1,0:T(8,128)(2,1)} %shard_map.137.refs_3_, ...), custom_call_target="tpu_custom_call" | custom-call | flops 12884901888 | bytes 8000000 | tf_op jit(solution)/shard_map/pallas_call | solution.py:498
  258.1 8.3 %shard_map.141.mine_b = bf16[1024,1024]{1,0:T(8,128)(2,1)S(1)} custom-call(s32[4]{0:T(128)S(1)} %copy-done.5, bf16[1024,2048]{1,0:T(8,128)(2,1)S(1)} %copy-done.8, bf16[16,64,1024]{2,1,0:T(8,128)(2,1)} %collective-permute-done.31.refs_2_, bf16[16,64,1024]{2,1,0:T(8,128)(2,1)} %collective-permute-done.32.refs_3_), custom_call_target="tpu_custom_call" | custom-call | flops 4294967296 | bytes 8000000 | tf_op jit(solution)/shard_map/pallas_call | solution.py:480
  266.4 20.1 %collective-permute-start.33 = (bf16[1024,1024]{1,0:T(8,128)(2,1)S(1)}, bf16[1024,1024]{1,0:T(8,128)(2,1)S(1)}, u32[]{:S(2)}, u32[]{:S(2)}) collective-permute-start(bf16[1024,1024]{1,0:T(8,128)(2,1)S(1)} %shard_map.141.mine_b), channel_id=1, source_target_pairs={{0,1},{1,0},{2,3},{3,2},{4,5},{5,4},{6,7},{7,6},{8,9},{9,8},{10,11... | collective-permute-start | bytes 6291464 | tf_op jit(solution)/shard_map/ppermute | solution.py:29
  286.8 3.5 %collective-permute-done.33.theirs_b = bf16[1024,1024]{1,0:T(8,128)(2,1)S(1)} collective-permute-done((bf16[1024,1024]{1,0:T(8,128)(2,1)S(1)}, bf16[1024,1024]{1,0:T(8,128)(2,1)S(1)}, u32[]{:S(2)}, u32[]{:S(2)}) %collective-permute-start.33) | collective-permute-done | bytes 2097184 | tf_op jit(solution)/shard_map/ppermute | solution.py:29
  293.3 4.8 %shard_map.142 = bf16[1024,1024]{1,0:T(8,128)(2,1)} custom-call(s32[4]{0:T(128)S(1)} %copy-done.5, bf16[1024,2048]{1,0:T(8,128)(2,1)S(1)} %copy-done, bf16[1024,1024]{1,0:T(8,128)(2,1)S(1)} %copy-done.3, bf16[1024,1024]{1,0:T(8,128)(2,1)S(1)} %collective-permute-done.30.theirs_a, bf16[1024,1024]{1,0:T(8,128)(2,1)S(1)} %shard_map.141.mine_b, ...), custom_call_target="tpu_custom_call" | custom-call | flops 2000000000 | bytes 8000000 | tf_op jit(solution)/shard_map/pallas_call | solution.py:524
  (119 shorter events, 60.1 us)
Async XLA Ops:
  10.1 12.0 %collective-permute-start.1 = (bf16[1,64,1792]{2,1,0:T(8,128)(2,1)S(1)}, bf16[1,64,1792]{2,1,0:T(8,128)(2,1)S(1)}, u32[]{:S(2)}, u32[]{:S(2)}) collective-permute-start(bf16[1,64,1792]{2,1,0:T(8,128)(2,1)S(1)} %maximum_bitcast_fusion.1), channel_id=1, source_target_pairs={{0,2},{2,4},{4,6},{6,0},{1,3},{3,5},{5,7},{7,1},{8,10},{10,12},{12... | collective-permute-start | bytes 688136 | tf_op jit(solution)/shard_map/ppermute | solution.py:29
  17.6 19.9 %collective-permute-start.11 = (bf16[4,64,768]{2,1,0:T(8,128)(2,1)S(1)}, bf16[4,64,768]{2,1,0:T(8,128)(2,1)S(1)}, u32[]{:S(2)}, u32[]{:S(2)}) collective-permute-start(bf16[4,64,768]{2,1,0:T(8,128)(2,1)S(1)} %pad_maximum_fusion.9), channel_id=1, source_target_pairs={{0,2},{2,4},{4,6},{6,0},{1,3},{3,5},{5,7},{7,1},{8,10},{10,12},{12... | collective-permute-start | bytes 1179656 | tf_op jit(solution)/shard_map/ppermute | solution.py:29
  18.9 19.9 %collective-permute-start.12 = (bf16[4,64,768]{2,1,0:T(8,128)(2,1)S(1)}, bf16[4,64,768]{2,1,0:T(8,128)(2,1)S(1)}, u32[]{:S(2)}, u32[]{:S(2)}) collective-permute-start(bf16[4,64,768]{2,1,0:T(8,128)(2,1)S(1)} %pad_maximum_fusion.9), channel_id=1, source_target_pairs={{0,6},{2,0},{4,2},{6,4},{1,7},{3,1},{5,3},{7,5},{8,14},{10,8},{12,... | collective-permute-start | bytes 1179656 | tf_op jit(solution)/shard_map/ppermute | solution.py:29
  20.3 13.0 %collective-permute-start.2 = (bf16[1,64,1792]{2,1,0:T(8,128)(2,1)S(1)}, bf16[1,64,1792]{2,1,0:T(8,128)(2,1)S(1)}, u32[]{:S(2)}, u32[]{:S(2)}) collective-permute-start(bf16[1,64,1792]{2,1,0:T(8,128)(2,1)S(1)} %maximum_bitcast_fusion.1), channel_id=1, source_target_pairs={{0,6},{2,0},{4,2},{6,4},{1,7},{3,1},{5,3},{7,5},{8,14},{10,8},{12,... | collective-permute-start | bytes 688136 | tf_op jit(solution)/shard_map/ppermute | solution.py:29
  21.6 14.2 %collective-permute-start.3 = (bf16[1,64,1792]{2,1,0:T(8,128)(2,1)S(1)}, bf16[1,64,1792]{2,1,0:T(8,128)(2,1)S(1)}, u32[]{:S(2)}, u32[]{:S(2)}) collective-permute-start(bf16[1,64,1792]{2,1,0:T(8,128)(2,1)S(1)} %maximum_bitcast_fusion.1), channel_id=1, source_target_pairs={{0,4},{2,6},{4,0},{6,2},{1,5},{3,7},{5,1},{7,3},{8,12},{10,14},{12... | collective-permute-start | bytes 688136 | tf_op jit(solution)/shard_map/ppermute | solution.py:29
  22.2 33.1 %collective-permute-start = (bf16[1024,1024]{1,0:T(8,128)(2,1)S(1)}, bf16[1024,1024]{1,0:T(8,128)(2,1)}, u32[]{:S(2)}, u32[]{:S(2)}) collective-permute-start(bf16[1024,1024]{1,0:T(8,128)(2,1)S(1)} %bitcast.27), channel_id=1, source_target_pairs={{0,1},{1,0},{2,3},{3,2},{4,5},{5,4},{6,7},{7,6},{8,9},{9,8},{10,11... | collective-permute-start | bytes 6291464 | tf_op jit(solution)/shard_map/ppermute | solution.py:29
  43.3 25.8 %collective-permute-start.14 = (bf16[16,64,768]{2,1,0:T(8,128)(2,1)}, bf16[16,64,768]{2,1,0:T(8,128)(2,1)}, u32[]{:S(2)}, u32[]{:S(2)}) collective-permute-start(bf16[16,64,768]{2,1,0:T(8,128)(2,1)} %pad_maximum_fusion.1.refs_9_.refs_13_), channel_id=1, source_target_pairs={{0,96},{32,0},{64,32},{96,64},{1,97},{33,1},{65,33},{97,65},{2,98}... | collective-permute-start | bytes 4718600 | tf_op jit(solution)/shard_map/ppermute | solution.py:29
  50.9 30.5 %collective-permute-start.7 = (bf16[16,64,768]{2,1,0:T(8,128)(2,1)}, bf16[16,64,768]{2,1,0:T(8,128)(2,1)}, u32[]{:S(2)}, u32[]{:S(2)}) collective-permute-start(bf16[16,64,768]{2,1,0:T(8,128)(2,1)} %pad_maximum_fusion.refs_7_.refs_11_), channel_id=1, source_target_pairs={{0,32},{32,64},{64,96},{96,0},{1,33},{33,65},{65,97},{97,1},{2,34}... | collective-permute-start | bytes 4718600 | tf_op jit(solution)/shard_map/ppermute | solution.py:29
  106.8 122.7 %collective-permute-start.15 = (bf16[2,1024,1024]{2,1,0:T(8,128)(2,1)}, bf16[2,1024,1024]{2,1,0:T(8,128)(2,1)}, u32[]{:S(2)}, u32[]{:S(2)}) collective-permute-start(bf16[2,1024,1024]{2,1,0:T(8,128)(2,1)} %shard_map.137.refs_3_), channel_id=1, source_target_pairs={{0,1},{1,0},{2,3},{3,2},{4,5},{5,4},{6,7},{7,6},{8,9},{9,8},{10,11... | collective-permute-start | bytes 12582920 | tf_op jit(solution)/shard_map/ppermute | solution.py:29
  122.6 19.6 %collective-permute-start.18 = (bf16[6,64,1024]{2,1,0:T(8,128)(2,1)S(1)}, bf16[6,64,1024]{2,1,0:T(8,128)(2,1)S(1)}, u32[]{:S(2)}, u32[]{:S(2)}) collective-permute-start(bf16[6,64,1024]{2,1,0:T(8,128)(2,1)S(1)} %fusion.1.refs_0_), channel_id=1, source_target_pairs={{0,8},{8,16},{16,24},{24,0},{1,9},{9,17},{17,25},{25,1},{2,10},{10... | collective-permute-start | bytes 2359304 | tf_op jit(solution)/shard_map/ppermute | solution.py:29
  123.3 25.2 %collective-permute-start.19 = (bf16[6,64,1024]{2,1,0:T(8,128)(2,1)S(1)}, bf16[6,64,1024]{2,1,0:T(8,128)(2,1)S(1)}, u32[]{:S(2)}, u32[]{:S(2)}) collective-permute-start(bf16[6,64,1024]{2,1,0:T(8,128)(2,1)S(1)} %fusion.1.refs_0_), channel_id=1, source_target_pairs={{0,24},{8,0},{16,8},{24,16},{1,25},{9,1},{17,9},{25,17},{2,26},{10... | collective-permute-start | bytes 2359304 | tf_op jit(solution)/shard_map/ppermute | solution.py:29
  125.3 33.5 %collective-permute-start.20 = (bf16[6,64,1024]{2,1,0:T(8,128)(2,1)S(1)}, bf16[6,64,1024]{2,1,0:T(8,128)(2,1)S(1)}, u32[]{:S(2)}, u32[]{:S(2)}) collective-permute-start(bf16[6,64,1024]{2,1,0:T(8,128)(2,1)S(1)} %fusion.1.refs_0_), channel_id=1, source_target_pairs={{0,16},{8,24},{16,0},{24,8},{1,17},{9,25},{17,1},{25,9},{2,18},{10... | collective-permute-start | bytes 2359304 | tf_op jit(solution)/shard_map/ppermute | solution.py:29
  125.4 38.1 %collective-permute-start.24 = (bf16[6,64,1024]{2,1,0:T(8,128)(2,1)S(1)}, bf16[6,64,1024]{2,1,0:T(8,128)(2,1)S(1)}, u32[]{:S(2)}, u32[]{:S(2)}) collective-permute-start(bf16[6,64,1024]{2,1,0:T(8,128)(2,1)S(1)} %fusion.refs_0_), channel_id=1, source_target_pairs={{0,2},{2,4},{4,6},{6,0},{1,3},{3,5},{5,7},{7,1},{8,10},{10,12},{12... | collective-permute-start | bytes 2359304 | tf_op jit(solution)/shard_map/ppermute | solution.py:29
  142.2 23.7 %collective-permute-start.25 = (bf16[6,64,1024]{2,1,0:T(8,128)(2,1)S(1)}, bf16[6,64,1024]{2,1,0:T(8,128)(2,1)S(1)}, u32[]{:S(2)}, u32[]{:S(2)}) collective-permute-start(bf16[6,64,1024]{2,1,0:T(8,128)(2,1)S(1)} %fusion.refs_0_), channel_id=1, source_target_pairs={{0,6},{2,0},{4,2},{6,4},{1,7},{3,1},{5,3},{7,5},{8,14},{10,8},{12,... | collective-permute-start | bytes 2359304 | tf_op jit(solution)/shard_map/ppermute | solution.py:29
  148.5 21.9 %collective-permute-start.26 = (bf16[6,64,1024]{2,1,0:T(8,128)(2,1)S(1)}, bf16[6,64,1024]{2,1,0:T(8,128)(2,1)S(1)}, u32[]{:S(2)}, u32[]{:S(2)}) collective-permute-start(bf16[6,64,1024]{2,1,0:T(8,128)(2,1)S(1)} %fusion.refs_0_), channel_id=1, source_target_pairs={{0,4},{2,6},{4,0},{6,2},{1,5},{3,7},{5,1},{7,3},{8,12},{10,14},{12... | collective-permute-start | bytes 2359304 | tf_op jit(solution)/shard_map/ppermute | solution.py:29
  159.2 39.1 %collective-permute-start.21 = (bf16[8,64,1024]{2,1,0:T(8,128)(2,1)S(1)}, bf16[8,64,1024]{2,1,0:T(8,128)(2,1)S(1)}, u32[]{:S(2)}, u32[]{:S(2)}) collective-permute-start(bf16[8,64,1024]{2,1,0:T(8,128)(2,1)S(1)} %get-tuple-element.12.refs_6_), channel_id=1, source_target_pairs={{0,2},{2,4},{4,6},{6,0},{1,3},{3,5},{5,7},{7,1},{8,10},{10,12},{12... | collective-permute-start | bytes 3145736 | tf_op jit(solution)/shard_map/ppermute | solution.py:29
  163.5 39.9 %collective-permute-start.22 = (bf16[8,64,1024]{2,1,0:T(8,128)(2,1)S(1)}, bf16[8,64,1024]{2,1,0:T(8,128)(2,1)S(1)}, u32[]{:S(2)}, u32[]{:S(2)}) collective-permute-start(bf16[8,64,1024]{2,1,0:T(8,128)(2,1)S(1)} %get-tuple-element.12.refs_6_), channel_id=1, source_target_pairs={{0,6},{2,0},{4,2},{6,4},{1,7},{3,1},{5,3},{7,5},{8,14},{10,8},{12,... | collective-permute-start | bytes 3145736 | tf_op jit(solution)/shard_map/ppermute | solution.py:29
  165.8 42.7 %collective-permute-start.23 = (bf16[8,64,1024]{2,1,0:T(8,128)(2,1)S(1)}, bf16[8,64,1024]{2,1,0:T(8,128)(2,1)S(1)}, u32[]{:S(2)}, u32[]{:S(2)}) collective-permute-start(bf16[8,64,1024]{2,1,0:T(8,128)(2,1)S(1)} %get-tuple-element.12.refs_6_), channel_id=1, source_target_pairs={{0,4},{2,6},{4,0},{6,2},{1,5},{3,7},{5,1},{7,3},{8,12},{10,14},{12... | collective-permute-start | bytes 3145736 | tf_op jit(solution)/shard_map/ppermute | solution.py:29
  172.3 36.2 %collective-permute-start.27 = (bf16[8,64,1024]{2,1,0:T(8,128)(2,1)}, bf16[8,64,1024]{2,1,0:T(8,128)(2,1)S(1)}, u32[]{:S(2)}, u32[]{:S(2)}) collective-permute-start(bf16[8,64,1024]{2,1,0:T(8,128)(2,1)} %get-tuple-element.13.refs_10_), channel_id=1, source_target_pairs={{0,8},{8,16},{16,24},{24,0},{1,9},{9,17},{17,25},{25,1},{2,10},{10... | collective-permute-start | bytes 3145736 | tf_op jit(solution)/shard_map/ppermute | solution.py:29
  198.3 31.2 %collective-permute-start.28 = (bf16[8,64,1024]{2,1,0:T(8,128)(2,1)}, bf16[8,64,1024]{2,1,0:T(8,128)(2,1)}, u32[]{:S(2)}, u32[]{:S(2)}) collective-permute-start(bf16[8,64,1024]{2,1,0:T(8,128)(2,1)} %get-tuple-element.13.refs_10_), channel_id=1, source_target_pairs={{0,24},{8,0},{16,8},{24,16},{1,25},{9,1},{17,9},{25,17},{2,26},{10... | collective-permute-start | bytes 3145736 | tf_op jit(solution)/shard_map/ppermute | solution.py:29
  203.4 26.1 %collective-permute-start.29 = (bf16[8,64,1024]{2,1,0:T(8,128)(2,1)}, bf16[8,64,1024]{2,1,0:T(8,128)(2,1)}, u32[]{:S(2)}, u32[]{:S(2)}) collective-permute-start(bf16[8,64,1024]{2,1,0:T(8,128)(2,1)} %get-tuple-element.13.refs_10_), channel_id=1, source_target_pairs={{0,16},{8,24},{16,0},{24,8},{1,17},{9,25},{17,1},{25,9},{2,18},{10... | collective-permute-start | bytes 3145736 | tf_op jit(solution)/shard_map/ppermute | solution.py:29
  208.6 47.3 %collective-permute-start.31 = (bf16[16,64,1024]{2,1,0:T(8,128)(2,1)S(1)}, bf16[16,64,1024]{2,1,0:T(8,128)(2,1)}, u32[]{:S(2)}, u32[]{:S(2)}) collective-permute-start(bf16[16,64,1024]{2,1,0:T(8,128)(2,1)S(1)} %get-tuple-element.14.refs_14_), channel_id=1, source_target_pairs={{0,32},{32,64},{64,96},{96,0},{1,33},{33,65},{65,97},{97,1},{2,34}... | collective-permute-start | bytes 6291464 | tf_op jit(solution)/shard_map/ppermute | solution.py:29
  209.9 46.0 %collective-permute-start.32 = (bf16[16,64,1024]{2,1,0:T(8,128)(2,1)}, bf16[16,64,1024]{2,1,0:T(8,128)(2,1)}, u32[]{:S(2)}, u32[]{:S(2)}) collective-permute-start(bf16[16,64,1024]{2,1,0:T(8,128)(2,1)} %get-tuple-element.15.refs_15_), channel_id=1, source_target_pairs={{0,96},{32,0},{64,32},{96,64},{1,97},{33,1},{65,33},{97,65},{2,98}... | collective-permute-start | bytes 6291464 | tf_op jit(solution)/shard_map/ppermute | solution.py:29
  266.4 23.9 %collective-permute-start.33 = (bf16[1024,1024]{1,0:T(8,128)(2,1)S(1)}, bf16[1024,1024]{1,0:T(8,128)(2,1)S(1)}, u32[]{:S(2)}, u32[]{:S(2)}) collective-permute-start(bf16[1024,1024]{1,0:T(8,128)(2,1)S(1)} %shard_map.141.mine_b), channel_id=1, source_target_pairs={{0,1},{1,0},{2,3},{3,2},{4,5},{5,4},{6,7},{7,6},{8,9},{9,8},{10,11... | collective-permute-start | bytes 6291464 | tf_op jit(solution)/shard_map/ppermute | solution.py:29
  (32 other events, 480.4 us)

commit v3 on v2

--- a/solution.py
+++ b/solution.py
@@ -56,7 +56,8 @@
 
 def whole_ring(v, places, axis):
     pieces = ring_pieces(v, places, axis)
-    return jnp.concatenate([p for p, _ in pieces], axis=0), sum((q for _, q in pieces), [])
+    whole = jnp.concatenate([p for p, _ in pieces], axis=0)
+    return whole, sum((q for _, q in pieces), [])
 
 
 def start_weights(refs, layout, pos, target, sem, plane=None):
@@ -74,19 +75,6 @@
             pltpu.make_async_copy(
                 ref.at[b, :, source], target.at[pl.ds(at, ref.shape[1]), cols], sem
             ).start()
-
-
-def sort_kernel(*refs):
-    pieces, (down, up), sem = refs[:4], refs[4:6], refs[6]
-    copies = []
-    for k, piece in enumerate(pieces):
-        copies.append((piece.at[4:6], up.at[2 * k : 2 * k + 2], sem.at[2 * k]))
-        copies.append((piece.at[0:4], down.at[4 * k : 4 * k + 4], sem.at[2 * k + 1]))
-    copies = [pltpu.make_async_copy(*c) for c in copies]
-    for c in copies:
-        c.start()
-    for c in copies:
-        c.wait()
 
 
 def norm_kernel(own, other, gain, normed):
@@ -401,26 +389,10 @@
     x_pieces = [by_xy, (step(by_xy[0], "z", 1), moved(by_xy[1], "z", 1))]
     y_pieces = [by_yx, (step(by_yx[0], "z", 3), moved(by_yx[1], "z", 1))]
 
-    def later(ring, at, cols, axis):
-        both = jnp.concatenate([ring[:, :, wide:], pair[:, :, cols]], axis=0)
-        pieces = ring_pieces(both, at + places, axis)
-        block = both.shape[1:]
-        split = call(
-            sort_kernel,
-            (jax.ShapeDtypeStruct((16, *block), bf16), jax.ShapeDtypeStruct((8, *block), bf16)),
-            [HBM] * 4,
-            1e6,
-            [pltpu.SemaphoreType.DMA((8,))],
-            VMEM,
-            16,
-        )(*[v for v, _ in pieces])
-        return [
-            (v, sum((p[s] for _, p in pieces), []))
-            for v, s in zip(split, (slice(0, 4), slice(4, 6)))
-        ]
-
-    down_a, up_a = later(by_x, at_x, slice(0, mid_col), "y")
-    down_b, up_b = later(by_y, at_y, slice(mid_col, hidden), "x")
+    up_a = whole_ring(pair[:, :, :mid_col], places, "y")
+    up_b = whole_ring(pair[:, :, mid_col:], places, "x")
+    down_a = whole_ring(by_x[:, :, wide:], at_x, "y")
+    down_b = whole_ring(by_y[:, :, wide:], at_y, "x")
     up_x = ring_pieces(*up_a, "x")
     up_y = ring_pieces(*up_b, "y")
     far_a = (step(down_a[0], "z", 1), moved(down_a[1], "z", 1))
@@ -455,6 +427,7 @@
             pltpu.SemaphoreType.DMA,
         ],
         HBM,
+        40,
     )(
         pos,
         normed,

time: 299 us -> 300 us (level)
  waiting for transfers between devices: 120 us -> 132 us
  starting transfers between devices: 91.9 us -> 80.5 us
  other arithmetic: 5.86 us -> 9.23 us
    ppermute x34 -> x40, waiting for transfers between devices: 120 us -> 132 us  [step(): return lax.ppermute(v, over, [(i, (i + shift) % size) for i in range(size)])]
    ppermute x34 -> x40, starting transfers between devices: 91.9 us -> 80.5 us  [step(): return lax.ppermute(v, over, [(i, (i + shift) % size) for i in range(size)])]
    concatenate x4 -> x8, other arithmetic: 2.86 us -> 7.31 us  [whole_ring(): whole = jnp.concatenate([p for p, _ in pieces], axis=0)]
    unnamed x46 -> x60, local copies, waits for them, and re-layouts: 6.14 us -> 6.88 us
  transfers between devices with their start and end apart: 34 -> 40, of which waited for: 16 -> 20; matrix products, arithmetic and copies ran while one was open for 2% -> 3% of each run, Pallas kernels for 11% -> 10%
where the time goes in v3:
time: 300 us
  waiting for transfers between devices  132 us (44%)
  starting transfers between devices  80.5 us (27%)
  Pallas kernels  67.6 us (23%)
  local copies, waits for them, and re-layouts  9.5 us (3%)
  other arithmetic  9.23 us (3%)
    ppermute x40, waiting for transfers between devices, step(): return lax.ppermute(v, over, [(i, (i + shift) % size) for i in range(size)])  132 us
    ppermute x40, starting transfers between devices, step(): return lax.ppermute(v, over, [(i, (i + shift) % size) for i in range(size)])  80.5 us
    pallas_call x1, Pallas kernels, local(): call(functools.partial(ffn_kernel, la + lb, lc), (whole, shape((length, h...  26.3 us
    pallas_call x1, Pallas kernels, local(): call(functools.partial(mixer_kernel, la + lb, lc + ld), partial, [SMEM] +...  25.1 us
    pallas_call x1, Pallas kernels, turned(): call(functools.partial(turned_kernel, layout, plane), one_half, [SMEM, HB...  8.22 us
    concatenate x8, other arithmetic, whole_ring(): whole = jnp.concatenate([p for p, _ in pieces], axis=0)  7.31 us
    unnamed x60, local copies, waits for them, and re-layouts  6.88 us
  transfers between devices with their start and end apart: 40, of which 20 were waited for; matrix products, arithmetic and copies ran while one was open for 3% of the time, Pallas kernels for 10%

profile of v3, /device:TPU:1, one launch (start us, length us, event | category | flops | bytes accessed | tf_op | source)
XLA Modules:
  0.0 299.5 jit_solution(14867014851411006126)
XLA Ops:
  2.8 3.8 %collective-permute-start.10 = (bf16[1,64,1792]{2,1,0:T(8,128)(2,1)S(1)}, bf16[1,64,1792]{2,1,0:T(8,128)(2,1)S(1)}, u32[]{:S(2)}, u32[]{:S(2)}) collective-permute-start(bf16[1,64,1792]{2,1,0:T(8,128)(2,1)S(1)} %maximum_bitcast_fusion.2), channel_id=1, source_target_pairs={{0,16},{8,24},{16,0},{24,8},{1,17},{9,25},{17,1},{25,9},{2,18},{10... | collective-permute-start | bytes 688136 | tf_op jit(solution)/shard_map/ppermute | solution.py:29
  11.7 5.9 %collective-permute-done.8 = bf16[1,64,1792]{2,1,0:T(8,128)(2,1)S(1)} collective-permute-done((bf16[1,64,1792]{2,1,0:T(8,128)(2,1)S(1)}, bf16[1,64,1792]{2,1,0:T(8,128)(2,1)S(1)}, u32[]{:S(2)}, u32[]{:S(2)}) %collective-permute-start.8) | collective-permute-done | bytes 229408 | tf_op jit(solution)/shard_map/ppermute | solution.py:29
  24.2 9.1 %collective-permute-done.2 = bf16[1,64,1792]{2,1,0:T(8,128)(2,1)S(1)} collective-permute-done((bf16[1,64,1792]{2,1,0:T(8,128)(2,1)S(1)}, bf16[1,64,1792]{2,1,0:T(8,128)(2,1)S(1)}, u32[]{:S(2)}, u32[]{:S(2)}) %collective-permute-start.2) | collective-permute-done | bytes 229408 | tf_op jit(solution)/shard_map/ppermute | solution.py:29
  58.7 10.4 %collective-permute-done.14.refs_10_.refs_14_ = bf16[16,64,768]{2,1,0:T(8,128)(2,1)} collective-permute-done((bf16[16,64,768]{2,1,0:T(8,128)(2,1)}, bf16[16,64,768]{2,1,0:T(8,128)(2,1)}, u32[]{:S(2)}, u32[]{:S(2)}) %collective-permute-start.14) | collective-permute-done | bytes 1572896 | tf_op jit(solution)/shard_map/ppermute | solution.py:29
  69.1 12.3 %collective-permute-done.7.refs_8_.refs_12_ = bf16[16,64,768]{2,1,0:T(8,128)(2,1)} collective-permute-done((bf16[16,64,768]{2,1,0:T(8,128)(2,1)}, bf16[16,64,768]{2,1,0:T(8,128)(2,1)}, u32[]{:S(2)}, u32[]{:S(2)}) %collective-permute-start.7) | collective-permute-done | bytes 1572896 | tf_op jit(solution)/shard_map/ppermute | solution.py:29
  81.4 25.1 %shard_map.137.refs_3_ = bf16[2,1024,1024]{2,1,0:T(8,128)(2,1)} custom-call(s32[4]{0:T(128)S(1)} %pad_add_fusion.refs_0_.pos, bf16[1024,2048]{1,0:T(8,128)(2,1)} %copy-done.1, f32[4,512]{1,0:T(4,128)S(1)} %copy-done.9, bf16[2,256,256]{2,1,0:T(8,128)(2,1)S(1)} %copy-done.7, bf16[2,256,256]{2,1,0:T(8,128)(2,1)S(1)} %copy-done.8, f32[1,512]{1,0:T(1,128)S(1)} %bitcast.31, ...), custom_call_target="tpu_custom_call" | custom-call | flops 12000000000 | bytes 8000000 | tf_op jit(solution)/shard_map/pallas_call | solution.py:411
  106.5 9.3 %collective-permute-start.15 = (bf16[2,1024,1024]{2,1,0:T(8,128)(2,1)}, bf16[2,1024,1024]{2,1,0:T(8,128)(2,1)}, u32[]{:S(2)}, u32[]{:S(2)}) collective-permute-start(bf16[2,1024,1024]{2,1,0:T(8,128)(2,1)} %shard_map.137.refs_3_), channel_id=1, source_target_pairs={{0,1},{1,0},{2,3},{3,2},{4,5},{5,4},{6,7},{7,6},{8,9},{9,8},{10,11... | collective-permute-start | bytes 12582920 | tf_op jit(solution)/shard_map/ppermute | solution.py:29
  125.0 4.2 %collective-permute-start.24 = (bf16[2,64,1024]{2,1,0:T(8,128)(2,1)S(1)}, bf16[2,64,1024]{2,1,0:T(8,128)(2,1)S(1)}, u32[]{:S(2)}, u32[]{:S(2)}) collective-permute-start(bf16[2,64,1024]{2,1,0:T(8,128)(2,1)S(1)} %get-tuple-element.11), channel_id=1, source_target_pairs={{0,2},{2,4},{4,6},{6,0},{1,3},{3,5},{5,7},{7,1},{8,10},{10,12},{12... | collective-permute-start | bytes 786440 | tf_op jit(solution)/shard_map/ppermute | solution.py:29
  136.0 6.2 %collective-permute-start.25 = (bf16[2,64,1024]{2,1,0:T(8,128)(2,1)S(1)}, bf16[2,64,1024]{2,1,0:T(8,128)(2,1)S(1)}, u32[]{:S(2)}, u32[]{:S(2)}) collective-permute-start(bf16[2,64,1024]{2,1,0:T(8,128)(2,1)S(1)} %get-tuple-element.11), channel_id=1, source_target_pairs={{0,6},{2,0},{4,2},{6,4},{1,7},{3,1},{5,3},{7,5},{8,14},{10,8},{12,... | collective-permute-start | bytes 786440 | tf_op jit(solution)/shard_map/ppermute | solution.py:29
  142.3 6.1 %collective-permute-done.25 = bf16[2,64,1024]{2,1,0:T(8,128)(2,1)S(1)} collective-permute-done((bf16[2,64,1024]{2,1,0:T(8,128)(2,1)S(1)}, bf16[2,64,1024]{2,1,0:T(8,128)(2,1)S(1)}, u32[]{:S(2)}, u32[]{:S(2)}) %collective-permute-start.25) | collective-permute-done | bytes 262176 | tf_op jit(solution)/shard_map/ppermute | solution.py:29
  148.3 4.9 %collective-permute-start.32 = (bf16[4,64,1024]{2,1,0:T(8,128)(2,1)S(1)}, bf16[4,64,1024]{2,1,0:T(8,128)(2,1)S(1)}, u32[]{:S(2)}, u32[]{:S(2)}) collective-permute-start(bf16[4,64,1024]{2,1,0:T(8,128)(2,1)S(1)} %pad_maximum_fusion.9), channel_id=1, source_target_pairs={{0,16},{8,24},{16,0},{24,8},{1,17},{9,25},{17,1},{25,9},{2,18},{10... | collective-permute-start | bytes 1572872 | tf_op jit(solution)/shard_map/ppermute | solution.py:29
  153.3 3.6 %collective-permute-start.34 = (bf16[4,64,1024]{2,1,0:T(8,128)(2,1)S(1)}, bf16[4,64,1024]{2,1,0:T(8,128)(2,1)S(1)}, u32[]{:S(2)}, u32[]{:S(2)}) collective-permute-start(bf16[4,64,1024]{2,1,0:T(8,128)(2,1)S(1)} %pad_maximum_fusion.6), channel_id=1, source_target_pairs={{0,6},{2,0},{4,2},{6,4},{1,7},{3,1},{5,3},{7,5},{8,14},{10,8},{12,... | collective-permute-start | bytes 1572872 | tf_op jit(solution)/shard_map/ppermute | solution.py:29
  158.2 4.0 %collective-permute-done.32 = bf16[4,64,1024]{2,1,0:T(8,128)(2,1)S(1)} collective-permute-done((bf16[4,64,1024]{2,1,0:T(8,128)(2,1)S(1)}, bf16[4,64,1024]{2,1,0:T(8,128)(2,1)S(1)}, u32[]{:S(2)}, u32[]{:S(2)}) %collective-permute-start.32) | collective-permute-done | bytes 524320 | tf_op jit(solution)/shard_map/ppermute | solution.py:29
  162.3 4.4 %collective-permute-done.33 = bf16[4,64,1024]{2,1,0:T(8,128)(2,1)S(1)} collective-permute-done((bf16[4,64,1024]{2,1,0:T(8,128)(2,1)S(1)}, bf16[4,64,1024]{2,1,0:T(8,128)(2,1)S(1)}, u32[]{:S(2)}, u32[]{:S(2)}) %collective-permute-start.33) | collective-permute-done | bytes 524320 | tf_op jit(solution)/shard_map/ppermute | solution.py:29
  169.1 9.8 %collective-permute-done.35 = bf16[4,64,1024]{2,1,0:T(8,128)(2,1)S(1)} collective-permute-done((bf16[4,64,1024]{2,1,0:T(8,128)(2,1)S(1)}, bf16[4,64,1024]{2,1,0:T(8,128)(2,1)S(1)}, u32[]{:S(2)}, u32[]{:S(2)}) %collective-permute-start.35) | collective-permute-done | bytes 524320 | tf_op jit(solution)/shard_map/ppermute | solution.py:29
  181.6 19.3 %collective-permute-done.21.refs_7_ = bf16[8,64,1024]{2,1,0:T(8,128)(2,1)S(1)} collective-permute-done((bf16[8,64,1024]{2,1,0:T(8,128)(2,1)S(1)}, bf16[8,64,1024]{2,1,0:T(8,128)(2,1)S(1)}, u32[]{:S(2)}, u32[]{:S(2)}) %collective-permute-start.21) | collective-permute-done | bytes 1048608 | tf_op jit(solution)/shard_map/ppermute | solution.py:29
  200.9 3.6 %collective-permute-start.28 = (bf16[8,64,1024]{2,1,0:T(8,128)(2,1)}, bf16[8,64,1024]{2,1,0:T(8,128)(2,1)}, u32[]{:S(2)}, u32[]{:S(2)}) collective-permute-start(bf16[8,64,1024]{2,1,0:T(8,128)(2,1)} %pad_maximum_fusion.5.refs_10_), channel_id=1, source_target_pairs={{0,24},{8,0},{16,8},{24,16},{1,25},{9,1},{17,9},{25,17},{2,26},{10... | collective-permute-start | bytes 3145736 | tf_op jit(solution)/shard_map/ppermute | solution.py:29
  207.0 16.8 %collective-permute-done.23.refs_9_ = bf16[8,64,1024]{2,1,0:T(8,128)(2,1)S(1)} collective-permute-done((bf16[8,64,1024]{2,1,0:T(8,128)(2,1)S(1)}, bf16[8,64,1024]{2,1,0:T(8,128)(2,1)S(1)}, u32[]{:S(2)}, u32[]{:S(2)}) %collective-permute-start.23) | collective-permute-done | bytes 1048608 | tf_op jit(solution)/shard_map/ppermute | solution.py:29
  228.7 26.3 %shard_map.138 = (bf16[1024,2048]{1,0:T(8,128)(2,1)}, bf16[1024,2048]{1,0:T(8,128)(2,1)}, bf16[1024,1024]{1,0:T(8,128)(2,1)}) custom-call(s32[4]{0:T(128)} %copy-done.5, bf16[1024,1024]{1,0:T(8,128)(2,1)} %bitcast.26, bf16[1024,1024]{1,0:T(8,128)(2,1)} %collective-permute-done.other.refs_2_, bf16[2,1024,1024]{2,1,0:T(8,128)(2,1)} %shard_map.137.refs_3_, ...), custom_call_target="tpu_custom_call" | custom-call | flops 12884901888 | bytes 8000000 | tf_op jit(solution)/shard_map/pallas_call | solution.py:471
  255.0 14.1 %collective-permute-done.37.refs_2_ = bf16[16,64,1024]{2,1,0:T(8,128)(2,1)S(1)} collective-permute-done((bf16[16,64,1024]{2,1,0:T(8,128)(2,1)}, bf16[16,64,1024]{2,1,0:T(8,128)(2,1)S(1)}, u32[]{:S(2)}, u32[]{:S(2)}) %collective-permute-start.37) | collective-permute-done | bytes 2097184 | tf_op jit(solution)/shard_map/ppermute | solution.py:29
  272.2 8.2 %shard_map.139.mine_b = bf16[1024,1024]{1,0:T(8,128)(2,1)S(1)} custom-call(s32[4]{0:T(128)S(1)} %copy-done.6, bf16[1024,2048]{1,0:T(8,128)(2,1)S(1)} %copy-done.10, bf16[16,64,1024]{2,1,0:T(8,128)(2,1)S(1)} %collective-permute-done.37.refs_2_, bf16[16,64,1024]{2,1,0:T(8,128)(2,1)} %collective-permute-done.38.refs_3_), custom_call_target="tpu_custom_call" | custom-call | flops 4294967296 | bytes 8000000 | tf_op jit(solution)/shard_map/pallas_call | solution.py:453
  280.4 7.4 %collective-permute-start.39 = (bf16[1024,1024]{1,0:T(8,128)(2,1)S(1)}, bf16[1024,1024]{1,0:T(8,128)(2,1)S(1)}, u32[]{:S(2)}, u32[]{:S(2)}) collective-permute-start(bf16[1024,1024]{1,0:T(8,128)(2,1)S(1)} %shard_map.139.mine_b), channel_id=1, source_target_pairs={{0,1},{1,0},{2,3},{3,2},{4,5},{5,4},{6,7},{7,6},{8,9},{9,8},{10,11... | collective-permute-start | bytes 6291464 | tf_op jit(solution)/shard_map/ppermute | solution.py:29
  287.9 3.7 %collective-permute-done.39.theirs_b = bf16[1024,1024]{1,0:T(8,128)(2,1)S(1)} collective-permute-done((bf16[1024,1024]{1,0:T(8,128)(2,1)S(1)}, bf16[1024,1024]{1,0:T(8,128)(2,1)S(1)}, u32[]{:S(2)}, u32[]{:S(2)}) %collective-permute-start.39) | collective-permute-done | bytes 2097184 | tf_op jit(solution)/shard_map/ppermute | solution.py:29
  294.6 4.8 %shard_map.140 = bf16[1024,1024]{1,0:T(8,128)(2,1)} custom-call(s32[4]{0:T(128)S(1)} %copy-done.6, bf16[1024,2048]{1,0:T(8,128)(2,1)S(1)} %copy-done, bf16[1024,1024]{1,0:T(8,128)(2,1)S(1)} %copy-done.3, bf16[1024,1024]{1,0:T(8,128)(2,1)S(1)} %collective-permute-done.36.theirs_a, bf16[1024,1024]{1,0:T(8,128)(2,1)S(1)} %shard_map.139.mine_b, ...), custom_call_target="tpu_custom_call" | custom-call | flops 2000000000 | bytes 8000000 | tf_op jit(solution)/shard_map/pallas_call | solution.py:497
  (147 shorter events, 75.7 us)
Async XLA Ops:
  17.6 19.9 %collective-permute-start.11 = (bf16[4,64,768]{2,1,0:T(8,128)(2,1)S(1)}, bf16[4,64,768]{2,1,0:T(8,128)(2,1)S(1)}, u32[]{:S(2)}, u32[]{:S(2)}) collective-permute-start(bf16[4,64,768]{2,1,0:T(8,128)(2,1)S(1)} %pad_maximum_fusion.12), channel_id=1, source_target_pairs={{0,2},{2,4},{4,6},{6,0},{1,3},{3,5},{5,7},{7,1},{8,10},{10,12},{12... | collective-permute-start | bytes 1179656 | tf_op jit(solution)/shard_map/ppermute | solution.py:29
  18.9 19.9 %collective-permute-start.12 = (bf16[4,64,768]{2,1,0:T(8,128)(2,1)S(1)}, bf16[4,64,768]{2,1,0:T(8,128)(2,1)S(1)}, u32[]{:S(2)}, u32[]{:S(2)}) collective-permute-start(bf16[4,64,768]{2,1,0:T(8,128)(2,1)S(1)} %pad_maximum_fusion.12), channel_id=1, source_target_pairs={{0,6},{2,0},{4,2},{6,4},{1,7},{3,1},{5,3},{7,5},{8,14},{10,8},{12,... | collective-permute-start | bytes 1179656 | tf_op jit(solution)/shard_map/ppermute | solution.py:29
  20.3 13.0 %collective-permute-start.2 = (bf16[1,64,1792]{2,1,0:T(8,128)(2,1)S(1)}, bf16[1,64,1792]{2,1,0:T(8,128)(2,1)S(1)}, u32[]{:S(2)}, u32[]{:S(2)}) collective-permute-start(bf16[1,64,1792]{2,1,0:T(8,128)(2,1)S(1)} %maximum_bitcast_fusion.1), channel_id=1, source_target_pairs={{0,6},{2,0},{4,2},{6,4},{1,7},{3,1},{5,3},{7,5},{8,14},{10,8},{12,... | collective-permute-start | bytes 688136 | tf_op jit(solution)/shard_map/ppermute | solution.py:29
  21.6 14.2 %collective-permute-start.3 = (bf16[1,64,1792]{2,1,0:T(8,128)(2,1)S(1)}, bf16[1,64,1792]{2,1,0:T(8,128)(2,1)S(1)}, u32[]{:S(2)}, u32[]{:S(2)}) collective-permute-start(bf16[1,64,1792]{2,1,0:T(8,128)(2,1)S(1)} %maximum_bitcast_fusion.1), channel_id=1, source_target_pairs={{0,4},{2,6},{4,0},{6,2},{1,5},{3,7},{5,1},{7,3},{8,12},{10,14},{12... | collective-permute-start | bytes 688136 | tf_op jit(solution)/shard_map/ppermute | solution.py:29
  22.2 31.3 %collective-permute-start = (bf16[1024,1024]{1,0:T(8,128)(2,1)S(1)}, bf16[1024,1024]{1,0:T(8,128)(2,1)}, u32[]{:S(2)}, u32[]{:S(2)}) collective-permute-start(bf16[1024,1024]{1,0:T(8,128)(2,1)S(1)} %bitcast.27), channel_id=1, source_target_pairs={{0,1},{1,0},{2,3},{3,2},{4,5},{5,4},{6,7},{7,6},{8,9},{9,8},{10,11... | collective-permute-start | bytes 6291464 | tf_op jit(solution)/shard_map/ppermute | solution.py:29
  43.3 25.8 %collective-permute-start.14 = (bf16[16,64,768]{2,1,0:T(8,128)(2,1)}, bf16[16,64,768]{2,1,0:T(8,128)(2,1)}, u32[]{:S(2)}, u32[]{:S(2)}) collective-permute-start(bf16[16,64,768]{2,1,0:T(8,128)(2,1)} %pad_maximum_fusion.3.refs_9_.refs_13_), channel_id=1, source_target_pairs={{0,96},{32,0},{64,32},{96,64},{1,97},{33,1},{65,33},{97,65},{2,98}... | collective-permute-start | bytes 4718600 | tf_op jit(solution)/shard_map/ppermute | solution.py:29
  50.9 30.5 %collective-permute-start.7 = (bf16[16,64,768]{2,1,0:T(8,128)(2,1)}, bf16[16,64,768]{2,1,0:T(8,128)(2,1)}, u32[]{:S(2)}, u32[]{:S(2)}) collective-permute-start(bf16[16,64,768]{2,1,0:T(8,128)(2,1)} %pad_maximum_fusion.2.refs_7_.refs_11_), channel_id=1, source_target_pairs={{0,32},{32,64},{64,96},{96,0},{1,33},{33,65},{65,97},{97,1},{2,34}... | collective-permute-start | bytes 4718600 | tf_op jit(solution)/shard_map/ppermute | solution.py:29
  106.5 122.1 %collective-permute-start.15 = (bf16[2,1024,1024]{2,1,0:T(8,128)(2,1)}, bf16[2,1024,1024]{2,1,0:T(8,128)(2,1)}, u32[]{:S(2)}, u32[]{:S(2)}) collective-permute-start(bf16[2,1024,1024]{2,1,0:T(8,128)(2,1)} %shard_map.137.refs_3_), channel_id=1, source_target_pairs={{0,1},{1,0},{2,3},{3,2},{4,5},{5,4},{6,7},{7,6},{8,9},{9,8},{10,11... | collective-permute-start | bytes 12582920 | tf_op jit(solution)/shard_map/ppermute | solution.py:29
  125.0 17.2 %collective-permute-start.24 = (bf16[2,64,1024]{2,1,0:T(8,128)(2,1)S(1)}, bf16[2,64,1024]{2,1,0:T(8,128)(2,1)S(1)}, u32[]{:S(2)}, u32[]{:S(2)}) collective-permute-start(bf16[2,64,1024]{2,1,0:T(8,128)(2,1)S(1)} %get-tuple-element.11), channel_id=1, source_target_pairs={{0,2},{2,4},{4,6},{6,0},{1,3},{3,5},{5,7},{7,1},{8,10},{10,12},{12... | collective-permute-start | bytes 786440 | tf_op jit(solution)/shard_map/ppermute | solution.py:29
  130.6 22.7 %collective-permute-start.30 = (bf16[4,64,1024]{2,1,0:T(8,128)(2,1)S(1)}, bf16[4,64,1024]{2,1,0:T(8,128)(2,1)S(1)}, u32[]{:S(2)}, u32[]{:S(2)}) collective-permute-start(bf16[4,64,1024]{2,1,0:T(8,128)(2,1)S(1)} %pad_maximum_fusion.9), channel_id=1, source_target_pairs={{0,8},{8,16},{16,24},{24,0},{1,9},{9,17},{17,25},{25,1},{2,10},{10... | collective-permute-start | bytes 1572872 | tf_op jit(solution)/shard_map/ppermute | solution.py:29
  130.6 26.3 %collective-permute-start.31 = (bf16[4,64,1024]{2,1,0:T(8,128)(2,1)S(1)}, bf16[4,64,1024]{2,1,0:T(8,128)(2,1)S(1)}, u32[]{:S(2)}, u32[]{:S(2)}) collective-permute-start(bf16[4,64,1024]{2,1,0:T(8,128)(2,1)S(1)} %pad_maximum_fusion.9), channel_id=1, source_target_pairs={{0,24},{8,0},{16,8},{24,16},{1,25},{9,1},{17,9},{25,17},{2,26},{10... | collective-permute-start | bytes 1572872 | tf_op jit(solution)/shard_map/ppermute | solution.py:29
  136.0 12.3 %collective-permute-start.25 = (bf16[2,64,1024]{2,1,0:T(8,128)(2,1)S(1)}, bf16[2,64,1024]{2,1,0:T(8,128)(2,1)S(1)}, u32[]{:S(2)}, u32[]{:S(2)}) collective-permute-start(bf16[2,64,1024]{2,1,0:T(8,128)(2,1)S(1)} %get-tuple-element.11), channel_id=1, source_target_pairs={{0,6},{2,0},{4,2},{6,4},{1,7},{3,1},{5,3},{7,5},{8,14},{10,8},{12,... | collective-permute-start | bytes 786440 | tf_op jit(solution)/shard_map/ppermute | solution.py:29
  148.3 13.9 %collective-permute-start.32 = (bf16[4,64,1024]{2,1,0:T(8,128)(2,1)S(1)}, bf16[4,64,1024]{2,1,0:T(8,128)(2,1)S(1)}, u32[]{:S(2)}, u32[]{:S(2)}) collective-permute-start(bf16[4,64,1024]{2,1,0:T(8,128)(2,1)S(1)} %pad_maximum_fusion.9), channel_id=1, source_target_pairs={{0,16},{8,24},{16,0},{24,8},{1,17},{9,25},{17,1},{25,9},{2,18},{10... | collective-permute-start | bytes 1572872 | tf_op jit(solution)/shard_map/ppermute | solution.py:29
  153.3 13.4 %collective-permute-start.33 = (bf16[4,64,1024]{2,1,0:T(8,128)(2,1)S(1)}, bf16[4,64,1024]{2,1,0:T(8,128)(2,1)S(1)}, u32[]{:S(2)}, u32[]{:S(2)}) collective-permute-start(bf16[4,64,1024]{2,1,0:T(8,128)(2,1)S(1)} %pad_maximum_fusion.6), channel_id=1, source_target_pairs={{0,2},{2,4},{4,6},{6,0},{1,3},{3,5},{5,7},{7,1},{8,10},{10,12},{12... | collective-permute-start | bytes 1572872 | tf_op jit(solution)/shard_map/ppermute | solution.py:29
  153.3 15.8 %collective-permute-start.34 = (bf16[4,64,1024]{2,1,0:T(8,128)(2,1)S(1)}, bf16[4,64,1024]{2,1,0:T(8,128)(2,1)S(1)}, u32[]{:S(2)}, u32[]{:S(2)}) collective-permute-start(bf16[4,64,1024]{2,1,0:T(8,128)(2,1)S(1)} %pad_maximum_fusion.6), channel_id=1, source_target_pairs={{0,6},{2,0},{4,2},{6,4},{1,7},{3,1},{5,3},{7,5},{8,14},{10,8},{12,... | collective-permute-start | bytes 1572872 | tf_op jit(solution)/shard_map/ppermute | solution.py:29
  156.9 22.0 %collective-permute-start.35 = (bf16[4,64,1024]{2,1,0:T(8,128)(2,1)S(1)}, bf16[4,64,1024]{2,1,0:T(8,128)(2,1)S(1)}, u32[]{:S(2)}, u32[]{:S(2)}) collective-permute-start(bf16[4,64,1024]{2,1,0:T(8,128)(2,1)S(1)} %pad_maximum_fusion.6), channel_id=1, source_target_pairs={{0,4},{2,6},{4,0},{6,2},{1,5},{3,7},{5,1},{7,3},{8,12},{10,14},{12... | collective-permute-start | bytes 1572872 | tf_op jit(solution)/shard_map/ppermute | solution.py:29
  162.3 38.6 %collective-permute-start.21 = (bf16[8,64,1024]{2,1,0:T(8,128)(2,1)S(1)}, bf16[8,64,1024]{2,1,0:T(8,128)(2,1)S(1)}, u32[]{:S(2)}, u32[]{:S(2)}) collective-permute-start(bf16[8,64,1024]{2,1,0:T(8,128)(2,1)S(1)} %pad_maximum_fusion.4.refs_6_), channel_id=1, source_target_pairs={{0,2},{2,4},{4,6},{6,0},{1,3},{3,5},{5,7},{7,1},{8,10},{10,12},{12... | collective-permute-start | bytes 3145736 | tf_op jit(solution)/shard_map/ppermute | solution.py:29
  166.7 37.9 %collective-permute-start.22 = (bf16[8,64,1024]{2,1,0:T(8,128)(2,1)S(1)}, bf16[8,64,1024]{2,1,0:T(8,128)(2,1)S(1)}, u32[]{:S(2)}, u32[]{:S(2)}) collective-permute-start(bf16[8,64,1024]{2,1,0:T(8,128)(2,1)S(1)} %pad_maximum_fusion.4.refs_6_), channel_id=1, source_target_pairs={{0,6},{2,0},{4,2},{6,4},{1,7},{3,1},{5,3},{7,5},{8,14},{10,8},{12,... | collective-permute-start | bytes 3145736 | tf_op jit(solution)/shard_map/ppermute | solution.py:29
  169.1 54.8 %collective-permute-start.23 = (bf16[8,64,1024]{2,1,0:T(8,128)(2,1)S(1)}, bf16[8,64,1024]{2,1,0:T(8,128)(2,1)S(1)}, u32[]{:S(2)}, u32[]{:S(2)}) collective-permute-start(bf16[8,64,1024]{2,1,0:T(8,128)(2,1)S(1)} %pad_maximum_fusion.4.refs_6_), channel_id=1, source_target_pairs={{0,4},{2,6},{4,0},{6,2},{1,5},{3,7},{5,1},{7,3},{8,12},{10,14},{12... | collective-permute-start | bytes 3145736 | tf_op jit(solution)/shard_map/ppermute | solution.py:29
  178.9 44.9 %collective-permute-start.27 = (bf16[8,64,1024]{2,1,0:T(8,128)(2,1)}, bf16[8,64,1024]{2,1,0:T(8,128)(2,1)S(1)}, u32[]{:S(2)}, u32[]{:S(2)}) collective-permute-start(bf16[8,64,1024]{2,1,0:T(8,128)(2,1)} %pad_maximum_fusion.5.refs_10_), channel_id=1, source_target_pairs={{0,8},{8,16},{16,24},{24,0},{1,9},{9,17},{17,25},{25,1},{2,10},{10... | collective-permute-start | bytes 3145736 | tf_op jit(solution)/shard_map/ppermute | solution.py:29
  200.9 27.8 %collective-permute-start.28 = (bf16[8,64,1024]{2,1,0:T(8,128)(2,1)}, bf16[8,64,1024]{2,1,0:T(8,128)(2,1)}, u32[]{:S(2)}, u32[]{:S(2)}) collective-permute-start(bf16[8,64,1024]{2,1,0:T(8,128)(2,1)} %pad_maximum_fusion.5.refs_10_), channel_id=1, source_target_pairs={{0,24},{8,0},{16,8},{24,16},{1,25},{9,1},{17,9},{25,17},{2,26},{10... | collective-permute-start | bytes 3145736 | tf_op jit(solution)/shard_map/ppermute | solution.py:29
  204.5 24.1 %collective-permute-start.29 = (bf16[8,64,1024]{2,1,0:T(8,128)(2,1)}, bf16[8,64,1024]{2,1,0:T(8,128)(2,1)}, u32[]{:S(2)}, u32[]{:S(2)}) collective-permute-start(bf16[8,64,1024]{2,1,0:T(8,128)(2,1)} %pad_maximum_fusion.5.refs_10_), channel_id=1, source_target_pairs={{0,16},{8,24},{16,0},{24,8},{1,17},{9,25},{17,1},{25,9},{2,18},{10... | collective-permute-start | bytes 3145736 | tf_op jit(solution)/shard_map/ppermute | solution.py:29
  223.8 45.2 %collective-permute-start.37 = (bf16[16,64,1024]{2,1,0:T(8,128)(2,1)}, bf16[16,64,1024]{2,1,0:T(8,128)(2,1)S(1)}, u32[]{:S(2)}, u32[]{:S(2)}) collective-permute-start(bf16[16,64,1024]{2,1,0:T(8,128)(2,1)} %pad_maximum_fusion.refs_14_), channel_id=1, source_target_pairs={{0,32},{32,64},{64,96},{96,0},{1,33},{33,65},{65,97},{97,1},{2,34}... | collective-permute-start | bytes 6291464 | tf_op jit(solution)/shard_map/ppermute | solution.py:29
  225.8 44.2 %collective-permute-start.38 = (bf16[16,64,1024]{2,1,0:T(8,128)(2,1)}, bf16[16,64,1024]{2,1,0:T(8,128)(2,1)}, u32[]{:S(2)}, u32[]{:S(2)}) collective-permute-start(bf16[16,64,1024]{2,1,0:T(8,128)(2,1)} %pad_maximum_fusion.1.refs_15_), channel_id=1, source_target_pairs={{0,96},{32,0},{64,32},{96,64},{1,97},{33,1},{65,33},{97,65},{2,98}... | collective-permute-start | bytes 6291464 | tf_op jit(solution)/shard_map/ppermute | solution.py:29
  (45 other events, 687.8 us)
